TPU v7x, 128 devices: a whole 4x4x4 slice. The times are simulated.
128 devices in a mesh: fs: 16 (over z, x), tp: 8 (over y, core).
Axes of the slice: x: 4, y: 4, z: 4, core: 2. Of those that a mesh axis runs over, the one named last changes fastest.
Arguments:
- tokens: bfloat16 [32, 384, 2048], P('fs', None, 'tp'), may hold values from -20 to 20
- first_gain: float32 [2048], replicated, may hold values from 0.1 to 1.9
- first_gate: bfloat16 [2048, 5120], P('fs', 'tp'), may hold values from -0.125 to 0.125
- first_up: bfloat16 [2048, 5120], P('fs', 'tp'), may hold values from -0.125 to 0.125
- first_down: bfloat16 [5120, 2048], P('tp', 'fs'), may hold values from -0.078125 to 0.078125
- mixer_gain: float32 [2048], replicated, may hold values from 0.1 to 1.9
- conv_input: bfloat16 [2048, 1024], P('fs', 'tp'), may hold values from -0.125 to 0.125
- outer_gate: bfloat16 [2048, 1024], P('fs', 'tp'), may hold values from -0.125 to 0.125
- inner_gate: bfloat16 [2048, 1024], P('fs', 'tp'), may hold values from -0.125 to 0.125
- conv_taps: float32 [3, 1024], P(None, 'tp'), may hold values from -3.5 to 3.5
- mixer_out: bfloat16 [1024, 2048], P('tp', 'fs'), may hold values from -0.1875 to 0.1875
- second_gain: float32 [2048], replicated, may hold values from 0.1 to 1.9
- second_gate: bfloat16 [2048, 5120], P('fs', 'tp'), may hold values from -0.125 to 0.125
- second_up: bfloat16 [2048, 5120], P('fs', 'tp'), may hold values from -0.125 to 0.125
- second_down: bfloat16 [5120, 2048], P('tp', 'fs'), may hold values from -0.078125 to 0.078125
Outputs:
- layer_out: bfloat16 [32, 384, 2048], P('fs', None, 'tp')
All inputs are finite; a program needn't handle non-finite values.
Results may differ from a plain program's by a relative error of at most 0.015.
Values may be sent and summed in bfloat16 or wider, within the bound.
A program may use at most 64 MiB of HBM per device.

v0:
```python
import jax
import jax.numpy as jnp
from jax import lax
from jax.sharding import PartitionSpec as P

epsilon = 1e-05


def sent_together(arrays, axis, dim, along):
    ends, at = ([], 0)
    for a in arrays[:-1]:
        at += a.shape[along]
        ends.append(at)
    both = jnp.concatenate(arrays, axis=along)
    return tuple(jnp.split(lax.all_gather(both, axis, axis=dim, tiled=True), ends, axis=along))


def copy_for_each(value, axis):
    copies = jnp.broadcast_to(value, (lax.axis_size(axis), *value.shape))
    return lax.all_to_all(copies, axis, split_axis=0, concat_axis=0, tiled=True)


def joined_along(pieces, dim):
    shape = list(pieces.shape[1:])
    shape[dim] *= pieces.shape[0]
    return jnp.moveaxis(pieces, 0, dim).reshape(shape)


def gathered_copies(value, axis, dim):
    pieces = copy_for_each(value, axis)
    return joined_along(pieces, dim)


def norm_rows(stream, gain):
    whole = lax.all_gather(stream, "tp", axis=1, tiled=True)
    values = whole.astype(jnp.float32)
    scale = lax.rsqrt(jnp.mean(values * values, axis=1, keepdims=True) + epsilon)
    return (values * scale * gain).astype(jnp.bfloat16)


def add_rows(gathered, piece):
    return jnp.dot(gathered, piece, preferred_element_type=jnp.float32)


def ffn_inputs(gathered, gate_weight, up_weight):
    pieces = sent_together((gate_weight, up_weight), "fs", 0, 1)
    gate = add_rows(gathered, pieces[0])
    upward = add_rows(gathered, pieces[1])
    return (gate, upward)


def mixer_inputs(gathered, conv_input, outer_gate, inner_gate):
    pieces = sent_together((conv_input, outer_gate, inner_gate), "fs", 0, 1)
    conv_values = add_rows(gathered, pieces[0])
    outer = add_rows(gathered, pieces[1])
    inner = add_rows(gathered, pieces[2])
    return (conv_values, outer, inner)


def project_down(hidden, weight):
    partial_sum = jnp.dot(
        hidden, gathered_copies(weight, "fs", 1), preferred_element_type=jnp.float32
    )
    result = lax.psum_scatter(
        partial_sum.astype(jnp.bfloat16), "tp", scatter_dimension=1, tiled=True
    ).astype(jnp.float32)
    return result


def half_ffn(stream, gain, gate_weight, up_weight, down_weight):
    gathered = norm_rows(stream, gain)
    gate, upward = ffn_inputs(gathered, gate_weight, up_weight)
    hidden = (jax.nn.silu(gate) * upward).astype(jnp.bfloat16)
    branch = project_down(hidden, down_weight)
    return (stream.astype(jnp.float32) + 0.5 * branch).astype(jnp.bfloat16)


def conv_mixer(stream, seqs, gain, conv_input, outer_gate, inner_gate, conv_taps, mixer_out):
    gathered = norm_rows(stream, gain)
    conv_values, outer, inner = mixer_inputs(gathered, conv_input, outer_gate, inner_gate)
    gated_input = (inner * conv_values).reshape(seqs, -1, conv_values.shape[1])
    one_back = jnp.pad(gated_input, ((0, 0), (1, 0), (0, 0)))[:, :-1]
    two_back = jnp.pad(gated_input, ((0, 0), (2, 0), (0, 0)))[:, :-2]
    convolved = conv_taps[0] * two_back + conv_taps[1] * one_back + conv_taps[2] * gated_input
    mixed = (outer * convolved.reshape(conv_values.shape)).astype(jnp.bfloat16)
    branch = project_down(mixed, mixer_out)
    return (stream.astype(jnp.float32) + branch).astype(jnp.bfloat16)


def on_device(
    tokens,
    first_gain,
    first_gate,
    first_up,
    first_down,
    mixer_gain,
    conv_input,
    outer_gate,
    inner_gate,
    conv_taps,
    mixer_out,
    second_gain,
    second_gate,
    second_up,
    second_down,
):
    seqs, length, width = tokens.shape
    stream = tokens.reshape(seqs * length, width)
    stream = half_ffn(stream, first_gain, first_gate, first_up, first_down)
    stream = conv_mixer(
        stream, seqs, mixer_gain, conv_input, outer_gate, inner_gate, conv_taps, mixer_out
    )
    stream = half_ffn(stream, second_gain, second_gate, second_up, second_down)
    return stream.reshape(seqs, length, width)


def solution(mesh):
    in_specs = (
        P("fs", None, "tp"),
        P(),
        P("fs", "tp"),
        P("fs", "tp"),
        P("tp", "fs"),
        P(),
        P("fs", "tp"),
        P("fs", "tp"),
        P("fs", "tp"),
        P(None, "tp"),
        P("tp", "fs"),
        P(),
        P("fs", "tp"),
        P("fs", "tp"),
        P("tp", "fs"),
    )
    out_specs = P("fs", None, "tp")
    return jax.shard_map(
        on_device, mesh=mesh, in_specs=in_specs, out_specs=out_specs, check_vma=False
    )
```

profile of v0, /device:TPU:0, one launch (start us, length us, event | category | flops | bytes accessed | tf_op | source)
XLA Modules:
  0.0 431.1 jit_solution(13457404551450091952)
XLA Ops:
  6.5 0.7 all-gather.7.cloned.1.call-update
  7.3 0.0 all-gather.9.cloned.1.call-start
  7.3 1.7 pad_maximum_fusion
  9.1 1.1 copy.16
  10.1 1.9 broadcast_in_dim.6
  12.0 8.2 %all-to-all-start = ((bf16[16,640,128]{1,2,0:T(8,128)(2,1)}), bf16[16,640,128]{1,2,0:T(8,128)(2,1)}, u32[]{:S(2)}, u32[]{:S(2)}) async-start(bf16[16,640,128]{1,2,0:T(8,128)(2,1)} %broadcast_in_dim.6), calls=%async_computation | async-start | bytes 5242880 | tf_op jit(solution)/shard_map/all_to_all | solution.py:20
  20.2 0.0 reduce-scatter.4.cloned.1.call-start
  20.3 22.4 %all-gather.7.cloned.1.call-done = bf16[768,2048]{1,0:T(8,128)(2,1)} async-done(((bf16[768,256]{1,0:T(8,128)(2,1)}), bf16[768,2048]{1,0:T(8,128)(2,1)}) %all-gather.7.cloned.1.call-update) | async-done | bytes 3145744 | tf_op jit(solution)/shard_map/all_gather | solution.py:35
  42.7 2.7 fusion
  45.4 56.7 %all-gather.9.cloned.1.call-done = bf16[2048,1280]{1,0:T(8,128)(2,1)} async-done(((bf16[128,1280]{1,0:T(8,128)(2,1)}), bf16[2048,1280]{1,0:T(8,128)(2,1)}) %all-gather.9.cloned.1.call-update) | async-done | bytes 5242896 | tf_op jit(solution)/shard_map/all_gather | solution.py:15
  102.1 5.7 %fusion.15 = f32[768,640]{1,0:T(8,128)} fusion(bf16[2048,1280]{1,0:T(8,128)(2,1)} %all-gather.9.cloned.1.call-done, bf16[768,2048]{1,0:T(8,128)(2,1)S(1)} %copy-done.3, f32[2048]{0:T(1024)S(1)} %copy-done.15, f32[768]{0:T(1024)S(1)} %add_rsqrt_fusion.2), kind=kOutput, calls=%fused_computation.24 | convolution fusion | flops 2019557376 | bytes 7744512 | tf_op jit(solution)/shard_map/dot_general | solution.py:42
  107.8 10.7 %convolution_convert_fusion.1 = bf16[768,2048]{1,0:T(8,128)(2,1)} fusion(bf16[640,2048]{0,1:T(8,128)(2,1)} %bitcast.2, f32[768,640]{1,0:T(8,128)} %fusion.15, bf16[2048,1280]{1,0:T(8,128)(2,1)} %all-gather.9.cloned.1.call-done, bf16[768,2048]{1,0:T(8,128)(2,1)S(1)} %copy-done.3, f32[2048]{0:T(1024)S(1)} %copy-done.15, f32[768]{0:T(1024)S(1)} %add_rsqrt_fusion.2), kind=kOutput, calls=%fused_computation.16 | convolution fusion | flops 4037345280 | bytes 13511680 | tf_op jit(solution)/shard_map/dot_general | solution.py:61
  118.5 0.0 reduce-scatter.4.cloned.1.call-update
  118.6 0.0 all-gather.11.cloned.1.call-start
  118.6 35.6 %reduce-scatter.4.cloned.1.call-done = bf16[768,256]{1,0:T(8,128)(2,1)} async-done(((bf16[768,2048]{1,0:T(8,128)(2,1)}), bf16[768,256]{1,0:T(8,128)(2,1)}) %reduce-scatter.4.cloned.1.call-update) | async-done | bytes 393232 | tf_op jit(solution)/shard_map/reduce_scatter | solution.py:64
  154.2 1.9 add_convert_fusion.2
  156.1 0.0 all-gather.13.cloned.1.call-start
  156.2 0.6 pad_maximum_fusion.2
  156.9 0.1 copy.17
  157.0 0.9 broadcast_in_dim.7
  157.9 7.0 %all-to-all-start.1 = ((bf16[16,128,128]{1,2,0:T(8,128)(2,1)}), bf16[16,128,128]{1,2,0:T(8,128)(2,1)}, u32[]{:S(2)}, u32[]{:S(2)}) async-start(bf16[16,128,128]{1,2,0:T(8,128)(2,1)} %broadcast_in_dim.7), calls=%async_computation.2 | async-start | bytes 1048576 | tf_op jit(solution)/shard_map/all_to_all | solution.py:20
  164.9 0.2 reduce-scatter.6.cloned.1.call-start
  165.2 21.0 %all-gather.11.cloned.1.call-done = bf16[768,2048]{1,0:T(8,128)(2,1)} async-done(((bf16[768,256]{1,0:T(8,128)(2,1)}), bf16[768,2048]{1,0:T(8,128)(2,1)}) %all-gather.11.cloned.1.call-update) | async-done | bytes 3145744 | tf_op jit(solution)/shard_map/all_gather | solution.py:35
  186.2 2.7 fusion.3
  189.0 0.1 copy-done
  189.0 0.8 fusion.5
  189.8 43.1 %all-gather.13.cloned.1.call-done = bf16[2048,384]{1,0:T(8,128)(2,1)} async-done(((bf16[128,384]{1,0:T(8,128)(2,1)}), bf16[2048,384]{1,0:T(8,128)(2,1)}) %all-gather.13.cloned.1.call-update) | async-done | bytes 1572880 | tf_op jit(solution)/shard_map/all_gather | solution.py:15
  233.0 2.0 fusion.35
  235.0 2.0 convolution_multiply_fusion
  237.0 0.1 fusion.41
  237.1 6.2 %convolution_convert_fusion.2 = bf16[768,2048]{1,0:T(8,128)(2,1)} fusion(bf16[128,2048]{0,1:T(8,128)(2,1)} %bitcast.9, f32[768,128]{1,0:T(8,128)S(1)} %bitcast.28, bf16[768,2048]{1,0:T(8,128)(2,1)S(1)} %fusion.5, bf16[2048,384]{1,0:T(8,128)(2,1)} %all-gather.13.cloned.1.call-done), kind=kOutput, calls=%fused_computation.17 | convolution fusion | flops 807075840 | bytes 7733248 | tf_op jit(solution)/shard_map/dot_general | solution.py:61
  243.3 0.0 reduce-scatter.6.cloned.1.call-update
  243.3 0.0 all-gather.15.cloned.1.call-start
  243.4 35.3 %reduce-scatter.6.cloned.1.call-done = bf16[768,256]{1,0:T(8,128)(2,1)} async-done(((bf16[768,2048]{1,0:T(8,128)(2,1)}), bf16[768,256]{1,0:T(8,128)(2,1)}) %reduce-scatter.6.cloned.1.call-update) | async-done | bytes 393232 | tf_op jit(solution)/shard_map/reduce_scatter | solution.py:64
  278.7 1.8 add_convert_fusion.1
  280.6 0.0 all-gather.17.cloned.1.call-start
  280.6 0.7 pad_maximum_fusion.1
  281.4 0.2 copy.18
  281.6 1.9 broadcast_in_dim.8
  283.5 7.1 %all-to-all-start.2 = ((bf16[16,640,128]{1,2,0:T(8,128)(2,1)}), bf16[16,640,128]{1,2,0:T(8,128)(2,1)}, u32[]{:S(2)}, u32[]{:S(2)}) async-start(bf16[16,640,128]{1,2,0:T(8,128)(2,1)} %broadcast_in_dim.8), calls=%async_computation.4 | async-start | bytes 5242880 | tf_op jit(solution)/shard_map/all_to_all | solution.py:20
  290.6 0.3 reduce-scatter.8.cloned.1.call-start
  290.9 19.8 %all-gather.15.cloned.1.call-done = bf16[768,2048]{1,0:T(8,128)(2,1)} async-done(((bf16[768,256]{1,0:T(8,128)(2,1)}), bf16[768,2048]{1,0:T(8,128)(2,1)}) %all-gather.15.cloned.1.call-update) | async-done | bytes 3145744 | tf_op jit(solution)/shard_map/all_gather | solution.py:35
  310.7 2.7 fusion.6
  313.4 57.2 %all-gather.17.cloned.1.call-done = bf16[2048,1280]{1,0:T(8,128)(2,1)} async-done(((bf16[128,1280]{1,0:T(8,128)(2,1)}), bf16[2048,1280]{1,0:T(8,128)(2,1)}) %all-gather.17.cloned.1.call-update) | async-done | bytes 5242896 | tf_op jit(solution)/shard_map/all_gather | solution.py:15
  370.6 5.7 %fusion.11 = f32[768,640]{1,0:T(8,128)} fusion(bf16[2048,1280]{1,0:T(8,128)(2,1)} %all-gather.17.cloned.1.call-done, bf16[768,2048]{1,0:T(8,128)(2,1)S(1)} %copy-done.4, f32[2048]{0:T(1024)S(1)} %copy-done.16, f32[768]{0:T(1024)S(1)} %add_rsqrt_fusion), kind=kOutput, calls=%fused_computation.20 | convolution fusion | flops 2019557376 | bytes 7744512 | tf_op jit(solution)/shard_map/dot_general | solution.py:42
  376.3 10.7 %convolution_convert_fusion = bf16[768,2048]{1,0:T(8,128)(2,1)} fusion(bf16[640,2048]{0,1:T(8,128)(2,1)} %bitcast.11, f32[768,640]{1,0:T(8,128)} %fusion.11, bf16[2048,1280]{1,0:T(8,128)(2,1)} %all-gather.17.cloned.1.call-done, bf16[768,2048]{1,0:T(8,128)(2,1)S(1)} %copy-done.4, f32[2048]{0:T(1024)S(1)} %copy-done.16, f32[768]{0:T(1024)S(1)} %add_rsqrt_fusion), kind=kOutput, calls=%fused_computation.15 | convolution fusion | flops 4037345280 | bytes 13511680 | tf_op jit(solution)/shard_map/dot_general | solution.py:61
  387.0 35.7 %reduce-scatter.8.cloned.1.call-done = bf16[768,256]{1,0:T(8,128)(2,1)} async-done(((bf16[768,2048]{1,0:T(8,128)(2,1)}), bf16[768,256]{1,0:T(8,128)(2,1)}) %reduce-scatter.8.cloned.1.call-update) | async-done | bytes 393232 | tf_op jit(solution)/shard_map/reduce_scatter | solution.py:64
  422.7 1.9 add_convert_fusion
  (47 shorter events, 0.2 us)
Async XLA Ops:
  6.5 36.1 %all-gather.7.cloned.1.call-start = ((), (), s32[]{:S(2)}) async-start(), calls=%async_computation.6 | async-start | bytes 3538944 | tf_op jit(solution)/shard_map/all_gather | solution.py:35
  7.3 94.8 %all-gather.9.cloned.1.call-start = ((), (), s32[]{:S(2)}) async-start(), calls=%async_computation.7 | async-start | bytes 5570560 | tf_op jit(solution)/shard_map/all_gather | solution.py:15
  12.0 90.1 %copy-start.15 = (f32[2048]{0:T(1024)S(1)}, f32[2048]{0:T(1024)}, u32[]{:S(2)}) copy-start(f32[2048]{0:T(1024)} %param.16) | copy-start | bytes 24580
  12.0 95.8 %all-to-all-start = ((bf16[16,640,128]{1,2,0:T(8,128)(2,1)}), bf16[16,640,128]{1,2,0:T(8,128)(2,1)}, u32[]{:S(2)}, u32[]{:S(2)}) async-start(bf16[16,640,128]{1,2,0:T(8,128)(2,1)} %broadcast_in_dim.6), calls=%async_computation | async-start | bytes 5242880 | tf_op jit(solution)/shard_map/all_to_all | solution.py:20
  20.2 134.0 %reduce-scatter.4.cloned.1.call-start = ((), (), s32[]{:S(2)}) async-start(), calls=%async_computation.8 | async-start | bytes 3538944 | tf_op jit(solution)/shard_map/reduce_scatter | solution.py:64
  42.7 59.5 %copy-start.3 = (bf16[768,2048]{1,0:T(8,128)(2,1)S(1)}, bf16[768,2048]{1,0:T(8,128)(2,1)}, u32[]{:S(2)}) copy-start(bf16[768,2048]{1,0:T(8,128)(2,1)} %all-gather.7.cloned.1.call-done) | copy-start | bytes 9437188
  118.5 35.7 %copy-start.5 = (bf16[2,384,256]{2,1,0:T(8,128)(2,1)S(1)}, bf16[2,384,256]{2,1,0:T(8,128)(2,1)}, u32[]{:S(2)}) copy-start(bf16[2,384,256]{2,1,0:T(8,128)(2,1)} %param.15) | copy-start | bytes 1179652
  118.5 37.7 %copy-start.10 = (bf16[128,128]{1,0:T(8,128)(2,1)S(1)}, bf16[128,128]{1,0:T(8,128)(2,1)}, u32[]{:S(2)}) copy-start(bf16[128,128]{1,0:T(8,128)(2,1)} %param.23) | copy-start | bytes 98308
  118.5 37.7 %copy-start.11 = (bf16[128,128]{1,0:T(8,128)(2,1)S(1)}, bf16[128,128]{1,0:T(8,128)(2,1)}, u32[]{:S(2)}) copy-start(bf16[128,128]{1,0:T(8,128)(2,1)} %param.22) | copy-start | bytes 98308
  118.5 37.7 %copy-start.12 = (bf16[128,128]{1,0:T(8,128)(2,1)S(1)}, bf16[128,128]{1,0:T(8,128)(2,1)}, u32[]{:S(2)}) copy-start(bf16[128,128]{1,0:T(8,128)(2,1)} %param.21) | copy-start | bytes 98308
  118.5 38.3 %copy-start.9 = (bf16[128,128]{1,0:T(8,128)(2,1)S(1)}, bf16[128,128]{1,0:T(8,128)(2,1)}, u32[]{:S(2)}) copy-start(bf16[128,128]{1,0:T(8,128)(2,1)} %param.25) | copy-start | bytes 98308
  118.5 46.6 %copy-start.14 = (f32[3,128]{1,0:T(4,128)S(1)}, f32[3,128]{1,0:T(4,128)}, u32[]{:S(2)}) copy-start(f32[3,128]{1,0:T(4,128)} %param.24) | copy-start | bytes 4612
  118.5 70.4 %copy-start.13 = (f32[2048]{0:T(1024)S(1)}, f32[2048]{0:T(1024)}, u32[]{:S(2)}) copy-start(f32[2048]{0:T(1024)} %param.20) | copy-start | bytes 24580
  118.6 67.6 %all-gather.11.cloned.1.call-start = ((), (), s32[]{:S(2)}) async-start(), calls=%async_computation.9 | async-start | bytes 3538944 | tf_op jit(solution)/shard_map/all_gather | solution.py:35
  156.1 76.9 %all-gather.13.cloned.1.call-start = ((), (), s32[]{:S(2)}) async-start(), calls=%async_computation.10 | async-start | bytes 1671168 | tf_op jit(solution)/shard_map/all_gather | solution.py:15
  157.9 79.2 %all-to-all-start.1 = ((bf16[16,128,128]{1,2,0:T(8,128)(2,1)}), bf16[16,128,128]{1,2,0:T(8,128)(2,1)}, u32[]{:S(2)}, u32[]{:S(2)}) async-start(bf16[16,128,128]{1,2,0:T(8,128)(2,1)} %broadcast_in_dim.7), calls=%async_computation.2 | async-start | bytes 1048576 | tf_op jit(solution)/shard_map/all_to_all | solution.py:20
  164.9 113.8 %reduce-scatter.6.cloned.1.call-start = ((), (), s32[]{:S(2)}) async-start(), calls=%async_computation.11 | async-start | bytes 3538944 | tf_op jit(solution)/shard_map/reduce_scatter | solution.py:64
  186.2 2.8 copy-start
  243.3 35.4 %copy-start.1 = (bf16[768,256]{1,0:T(8,128)(2,1)S(1)}, bf16[768,256]{1,0:T(8,128)(2,1)}, u32[]{:S(2)}) copy-start(bf16[768,256]{1,0:T(8,128)(2,1)} %add_convert_fusion.2) | copy-start | bytes 1179652
  243.3 37.3 %copy-start.6 = (bf16[128,640]{1,0:T(8,128)(2,1)S(1)}, bf16[128,640]{1,0:T(8,128)(2,1)}, u32[]{:S(2)}) copy-start(bf16[128,640]{1,0:T(8,128)(2,1)} %param.28) | copy-start | bytes 491524
  243.3 37.3 %copy-start.7 = (bf16[128,640]{1,0:T(8,128)(2,1)S(1)}, bf16[128,640]{1,0:T(8,128)(2,1)}, u32[]{:S(2)}) copy-start(bf16[128,640]{1,0:T(8,128)(2,1)} %param.27) | copy-start | bytes 491524
  243.3 38.1 %copy-start.8 = (bf16[640,128]{1,0:T(8,128)(2,1)S(1)}, bf16[640,128]{1,0:T(8,128)(2,1)}, u32[]{:S(2)}) copy-start(bf16[640,128]{1,0:T(8,128)(2,1)} %param.29) | copy-start | bytes 491524
  243.3 67.3 %all-gather.15.cloned.1.call-start = ((), (), s32[]{:S(2)}) async-start(), calls=%async_computation.12 | async-start | bytes 3538944 | tf_op jit(solution)/shard_map/all_gather | solution.py:35
  280.6 90.0 %all-gather.17.cloned.1.call-start = ((), (), s32[]{:S(2)}) async-start(), calls=%async_computation.13 | async-start | bytes 5570560 | tf_op jit(solution)/shard_map/all_gather | solution.py:15
  283.5 87.1 %copy-start.16 = (f32[2048]{0:T(1024)S(1)}, f32[2048]{0:T(1024)}, u32[]{:S(2)}) copy-start(f32[2048]{0:T(1024)} %param.26) | copy-start | bytes 24580
  283.5 92.8 %all-to-all-start.2 = ((bf16[16,640,128]{1,2,0:T(8,128)(2,1)}), bf16[16,640,128]{1,2,0:T(8,128)(2,1)}, u32[]{:S(2)}, u32[]{:S(2)}) async-start(bf16[16,640,128]{1,2,0:T(8,128)(2,1)} %broadcast_in_dim.8), calls=%async_computation.4 | async-start | bytes 5242880 | tf_op jit(solution)/shard_map/all_to_all | solution.py:20
  290.6 132.1 %reduce-scatter.8.cloned.1.call-start = ((), (), s32[]{:S(2)}) async-start(), calls=%async_computation.14 | async-start | bytes 3538944 | tf_op jit(solution)/shard_map/reduce_scatter | solution.py:64
  310.7 60.0 %copy-start.4 = (bf16[768,2048]{1,0:T(8,128)(2,1)S(1)}, bf16[768,2048]{1,0:T(8,128)(2,1)}, u32[]{:S(2)}) copy-start(bf16[768,2048]{1,0:T(8,128)(2,1)} %all-gather.15.cloned.1.call-done) | copy-start | bytes 9437188
  387.0 35.7 %copy-start.2 = (bf16[768,256]{1,0:T(8,128)(2,1)S(1)}, bf16[768,256]{1,0:T(8,128)(2,1)}, u32[]{:S(2)}) copy-start(bf16[768,256]{1,0:T(8,128)(2,1)} %add_convert_fusion.1) | copy-start | bytes 1179652
Sparse Core Ops, SparseCore 0:
  9.0 33.5 all-gather.6
  44.8 57.2 all-gather.8
  118.7 35.4 reduce-scatter.3
  156.2 29.9 all-gather.10
  188.2 44.7 all-gather.12
  243.5 35.2 reduce-scatter.5
  280.7 29.9 all-gather.14
  312.8 57.7 all-gather.16
  387.1 35.4 reduce-scatter.7
where the time goes:
time: 432 us; the launch traced here: 431 us
  waiting for transfers between devices  328 us (76%)
  matrix products  42.9 us (10%)
  starting transfers between devices  23 us (5%)
  other arithmetic  17.8 us (4%)
  between operations  13.4 us (3%)
  local copies, waits for them, and re-layouts  6.23 us (1%)
    all_gather x3, waiting for transfers between devices, sent_together(): lax.all_gather(both, axis, axis=dim, tiled=True)  157 us
    reduce_scatter x3, waiting for transfers between devices, project_down(): lax.psum_scatter(partial_sum.astype(jnp.bfloat16), 'tp', scatter_dimensio...  107 us
    all_gather x3, waiting for transfers between devices, norm_rows(): whole = lax.all_gather(stream, 'tp', axis=1, tiled=True)  63.2 us
    dot_general x3, matrix products, project_down(): jnp.dot(hidden, gathered_copies(weight, 'fs', 1), preferred_element_type=...  27.5 us
    all_to_all x3, starting transfers between devices, copy_for_each(): return lax.all_to_all(copies, axis, split_axis=0, concat_axis=0, tiled=True)  22.3 us
    dot_general x4, matrix products, add_rows(): return jnp.dot(gathered, piece, preferred_element_type=jnp.float32)  15.4 us
  transfers between devices with their start and end apart: 12, of which 9 were waited for; matrix products, arithmetic and copies ran while one was open for 8% of the time, Pallas kernels for 0%

commit v1 on v0

v1 whole, which is shorter than its diff:
```python
import functools

import jax
import jax.numpy as jnp
from jax import lax
from jax.experimental import pallas as pl
from jax.experimental.pallas import tpu as pltpu
from jax.sharding import PartitionSpec as P

EPS = 1e-05
MESH = pl.DeviceIdType.MESH
F32, BF16 = jnp.float32, jnp.bfloat16

D = 2048
ROWS = 768
LEN = 384
BLK = 256
NC = 2
R = ROWS // NC
HALF = R // 2
SUB = 64
SLABS = 34
GROUPS = ((0, 10), (10, 5), (15, 4), (19, 10), (29, 5))
UNITS = (0, 2, 3, 4, 3, 2, 1)
AHEAD = (2, 1, 3, 0)


def schedule():
    order = [("W", 0, 0), ("G0", 0, 0), ("G0", 0, 1), ("W", 0, 1), ("G1", 0, 0), ("G1", 0, 1), ("W", 0, 2)]
    order += [("G2", 0, 0), ("G2", 0, 1), ("G3", 0, 0), ("N", 0, 0), ("G3", 0, 1), ("N", 0, 1)]
    order += [("W", 0, 3), ("W", 1, 0), ("W", 0, 4), ("W", 0, 5), ("W", 1, 1), ("F", 0, 0), ("W", 1, 2), ("F", 0, 1)]
    order += [("W", 1, 3), ("W", 2, 0), ("W", 1, 4), ("W", 1, 5), ("W", 2, 1)]
    order += [("DP", 0, 0), ("DO", 0, 0), ("SA", 0, 0), ("DP", 0, 1), ("DO", 0, 1), ("SA", 0, 1), ("W", 2, 2)]
    order += [("SB", 0, 0), ("SB", 0, 1), ("W", 2, 3), ("W", 3, 0), ("SC", 0, 0), ("W", 2, 4), ("SC", 0, 1), ("W", 2, 5)]
    order += [("G1", 1, 0), ("W", 3, 1), ("G2", 1, 0), ("G1", 1, 1), ("G3", 1, 0), ("N", 1, 0), ("F", 1, 0), ("DP", 1, 0)]
    order += [("DO", 1, 0), ("SA", 1, 0), ("G2", 1, 1), ("G3", 1, 1), ("N", 1, 1), ("F", 1, 1), ("SB", 1, 0), ("DP", 1, 1)]
    order += [("W", 3, 2), ("DO", 1, 1), ("SA", 1, 1), ("SC", 1, 0), ("SB", 1, 1), ("W", 3, 3), ("W", 4, 0), ("G1", 2, 0)]
    order += [("SC", 1, 1), ("G2", 2, 0), ("W", 3, 4), ("G1", 2, 1), ("G3", 2, 0), ("N", 2, 0), ("G2", 2, 1), ("W", 3, 5)]
    order += [("W", 4, 1), ("F", 2, 0), ("G3", 2, 1), ("N", 2, 1), ("F", 2, 1), ("W", 4, 2), ("W", 4, 3), ("W", 4, 4), ("W", 4, 5)]
    order += [("DP", 2, 0), ("DO", 2, 0), ("SA", 2, 0), ("DP", 2, 1), ("DO", 2, 1), ("SA", 2, 1)]
    order += [("SB", 2, 0), ("SB", 2, 1), ("SC", 2, 0), ("SC", 2, 1)]
    return order


def layer_kernel(
    tokens, gains, taps, fgate, fup, fdown, conv_in, outer_gate, inner_gate, mix_out, sgate, sup, sdown,
    out,
    w, xg, normed, hidden, psend, precv, pown, s1, r1, s2, r2, gi, outer_s, mixed, result,
    w_load, x_load, w_send, w_recv, y_send, g_recv, s_recv, o_sem,
):
    f, t = lax.axis_index("fs"), lax.axis_index("tp")
    z, x = f // 4, f % 4
    y, core = t // 2, t % 2
    other = 1 - core

    def slot(h, a, b):
        za, xa = (b, a) if h == 0 else (a, b)
        return ((z + za) % 4) * 4 + (x + xa) % 4

    def at_y(ahead, which):
        return ((y + ahead) % 4) * 2 + which

    def w_device(h, phase, d):
        return (slot(h, d, 0) if phase == 1 else slot(h, 0, d), t)

    up, down, partner = (f, at_y(1, core)), (f, at_y(3, core)), (f, at_y(0, other))

    def load_tokens():
        return pltpu.make_async_copy(tokens, xg.at[0, t], x_load)

    def loads(g):
        sources = []
        if g in (0, 3):
            for s in range(5):
                for a in (fgate, fup) if g == 0 else (sgate, sup):
                    sources.append(a.at[:, pl.ds(128 * s, 128)])
        elif g in (1, 4):
            a = fdown if g == 1 else sdown
            sources = [a.at[pl.ds(128 * s, 128), :] for s in range(5)]
        else:
            sources = [conv_in, outer_gate, inner_gate, mix_out]
        first = GROUPS[g][0]
        return [pltpu.make_async_copy(a, w.at[f, first + i], w_load.at[g]) for i, a in enumerate(sources)]

    def await_bytes(ref, sem):
        pltpu.make_async_copy(ref, ref, sem).wait()

    load_tokens().start()
    for g in range(5):
        for copy in loads(g):
            copy.start()

    barrier = pltpu.get_barrier_semaphore()
    peers = [w_device(h, 1, d) for h in (0, 1) for d in (1, 3)] + [up, down, partner]
    for peer in peers:
        pl.semaphore_signal(barrier, inc=1, device_id=peer, device_id_type=MESH)

    gi[:, pl.ds(0, 8), :] = jnp.zeros((2, 8, 128), F32)

    load_tokens().wait()
    pl.semaphore_wait(barrier, len(peers))

    def w_copy(g, h, a, b, phase, d, quarter, landing):
        first, count = GROUPS[g]
        if quarter:
            rows = pl.ds(64 * h + (0 if d == 1 else 32), 32)
        else:
            rows = pl.ds(64 * h, 64)
        part = w.at[slot(h, a, b), pl.ds(first, count), rows]
        pltpu.make_async_remote_copy(
            src_ref=part, dst_ref=part, send_sem=w_send.at[g], recv_sem=w_recv.at[g, landing],
            device_id=w_device(h, phase, d), device_id_type=MESH,
        ).start()

    def w_wait(g, landing):
        first, count = GROUPS[g]
        await_bytes(w.at[pl.ds(0, UNITS[landing]), pl.ds(first, count)], w_recv.at[g, landing])

    both = [(h, d) for h in (0, 1) for d in (1, 3)]

    def weights(g, rnd):
        first, count = GROUPS[g]
        if rnd == 0:
            await_bytes(w.at[f, pl.ds(first, count)], w_load.at[g])
            for h, d in both:
                w_copy(g, h, 0, 0, 1, d, False, 1)
            for h, d in both:
                w_copy(g, h, 0, 0, 2, d, False, 2)
        elif rnd == 5:
            w_wait(g, 5)
            w_wait(g, 6)
        else:
            w_wait(g, rnd)
            for h, d in both:
                back = 4 - d
                if rnd == 1:
                    w_copy(g, h, back, 0, 1, d, True, 2)
                    w_copy(g, h, 1, 0, 2, d, False, 3)
                    w_copy(g, h, 3, 0, 2, d, False, 3)
                elif rnd == 2:
                    w_copy(g, h, 0, back, 2, d, True, 4)
                    w_copy(g, h, 2, 0, 2, d, False, 4)
                elif rnd == 3:
                    w_copy(g, h, 1, back, 2, d, True, 5)
                    w_copy(g, h, 3, back, 2, d, True, 5)
                else:
                    w_copy(g, h, 2, back, 2, d, True, 6)

    def y_copy(src, dst, stage, c, recv, device):
        pltpu.make_async_remote_copy(
            src_ref=src, dst_ref=dst, send_sem=y_send.at[stage, c], recv_sem=recv,
            device_id=device, device_id_type=MESH,
        ).start()

    def rows_of(c):
        return pl.ds(c * R, R)

    def front(c):
        return pl.ds(c * R, HALF)

    def rear(c):
        return pl.ds(c * R + HALF, HALF)

    def gather_0(stage, c):
        mine = xg.at[stage, t, rows_of(c)]
        for device in (up, down):
            y_copy(mine, mine, stage, c, g_recv.at[stage, c, 0], device)
        y_copy(mine, mine, stage, c, g_recv.at[stage, c, 2], partner)

    def gather_1(stage, c):
        await_bytes(xg.at[stage, pl.ds(0, 2), rows_of(c)], g_recv.at[stage, c, 0])
        below, above = at_y(3, core), at_y(1, core)
        for block, part, device in ((below, front(c), up), (above, rear(c), down)):
            ref = xg.at[stage, block, part]
            y_copy(ref, ref, stage, c, g_recv.at[stage, c, 1], device)
        for block in (below, above):
            ref = xg.at[stage, block, rows_of(c)]
            y_copy(ref, ref, stage, c, g_recv.at[stage, c, 2], partner)

    def gather_2(stage, c):
        await_bytes(xg.at[stage, 0, rows_of(c)], g_recv.at[stage, c, 1])
        ref = xg.at[stage, at_y(2, core), rows_of(c)]
        y_copy(ref, ref, stage, c, g_recv.at[stage, c, 2], partner)

    def gather_3(stage, c):
        await_bytes(xg.at[stage, pl.ds(0, 4), rows_of(c)], g_recv.at[stage, c, 2])

    def norm(stage, c):
        @pl.loop(0, R // SUB)
        def _(i):
            rows = pl.ds(pl.multiple_of(c * R + i * SUB, SUB), SUB)
            total = jnp.zeros((SUB, BLK), F32)
            for b in range(8):
                v = xg[stage, b, rows, :].astype(F32)
                total = total + v * v
            mean = jnp.sum(total, axis=1, keepdims=True) * (1.0 / D)
            scale = lax.rsqrt(mean + EPS)
            for b in range(8):
                v = xg[stage, b, rows, :].astype(F32)
                cols = pl.ds(b * BLK, BLK)
                normed[rows, cols] = (v * scale * gains[stage : stage + 1, cols]).astype(BF16)

    def columns(first):
        return w[:, first].reshape(D, 128)

    def ffn(stage, c):
        first = 0 if stage == 0 else 19

        @pl.loop(0, 5)
        def _(s):
            pair = jnp.concatenate([columns(first + 2 * s), columns(first + 2 * s + 1)], axis=1)
            both_halves = jnp.dot(normed[rows_of(c), :], pair, preferred_element_type=F32)
            gate, upward = both_halves[:, :128], both_halves[:, 128:]
            value = gate / (1.0 + jnp.exp(-gate)) * upward
            hidden[rows_of(c), pl.ds(pl.multiple_of(128 * s, 128), 128)] = value.astype(BF16)

    def mixer(c):
        three = jnp.concatenate([columns(15), columns(16), columns(17)], axis=1)
        products = jnp.dot(normed[rows_of(c), :], three, preferred_element_type=F32)
        seq, at = c * R // LEN, c * R % LEN
        gi[seq, pl.ds(8 + at, R), :] = products[:, 256:] * products[:, :128]
        outer_s[...] = products[:, 128:256]
        convolved = taps[0:1, :] * gi[seq, pl.ds(6 + at, R), :]
        convolved = convolved + taps[1:2, :] * gi[seq, pl.ds(7 + at, R), :]
        convolved = convolved + taps[2:3, :] * gi[seq, pl.ds(8 + at, R), :]
        mixed[rows_of(c), :] = (outer_s[...] * convolved).astype(BF16)

    def product(stage, c, block):
        a, b = 2 * block, 2 * block + 1
        if stage == 1:
            pair = jnp.concatenate([w[a, 18], w[b, 18]], axis=1)
            return jnp.dot(mixed[rows_of(c), :], pair, preferred_element_type=F32)
        slabs = pl.ds(10 if stage == 0 else 29, 5)
        pair = jnp.concatenate([w[a, slabs].reshape(640, 128), w[b, slabs].reshape(640, 128)], axis=1)
        return jnp.dot(hidden[rows_of(c), :], pair, preferred_element_type=F32)

    def down_partner(stage, c):
        for i in range(4):
            psend[stage, i, rows_of(c), :] = product(stage, c, at_y(AHEAD[i], other)).astype(BF16)
        part = pl.ds(0, 4)
        y_copy(psend.at[stage, part, rows_of(c)], precv.at[stage, part, rows_of(c)], stage, c, s_recv.at[stage, c, 0], partner)

    def down_own(stage, c):
        for i in range(4):
            pown[i, rows_of(c), :] = product(stage, c, at_y(AHEAD[i], core))

    def pair_sum(stage, i, rows):
        return pown[i, rows, :] + precv[stage, i, rows, :].astype(F32)

    def over(first, count, body):
        @pl.loop(0, count // SUB)
        def _(i):
            body(pl.ds(pl.multiple_of(first + i * SUB, SUB), SUB))

    def sum_a(stage, c):
        await_bytes(precv.at[stage, pl.ds(0, 4), rows_of(c)], s_recv.at[stage, c, 0])

        def body(rows):
            s1[stage, rows, :] = pair_sum(stage, 0, rows).astype(BF16)

        over(c * R, R, body)
        for part, device in ((front(c), up), (rear(c), down)):
            y_copy(s1.at[stage, part], r1.at[stage, part], stage, c, s_recv.at[stage, c, 1], device)

    def sum_b(stage, c):
        await_bytes(r1.at[stage, rows_of(c)], s_recv.at[stage, c, 1])

        def with_r1(i, rows):
            value = pair_sum(stage, i, rows) + r1[stage, rows, :].astype(F32)
            s2[stage, i - 1, rows, :] = value.astype(BF16)

        def alone(i, rows):
            s2[stage, i - 1, rows, :] = pair_sum(stage, i, rows).astype(BF16)

        def front_body(rows):
            with_r1(1, rows)
            alone(2, rows)

        def rear_body(rows):
            alone(1, rows)
            with_r1(2, rows)

        over(c * R, HALF, front_body)
        over(c * R + HALF, HALF, rear_body)
        for i, device in ((0, up), (1, down)):
            y_copy(s2.at[stage, i, rows_of(c)], r2.at[stage, i, rows_of(c)], stage, c, s_recv.at[stage, c, 2], device)

    def sum_c(stage, c):
        await_bytes(r2.at[stage, pl.ds(0, 2), rows_of(c)], s_recv.at[stage, c, 2])

        def body(rows):
            branch = pair_sum(stage, 3, rows) + r2[stage, 0, rows, :].astype(F32) + r2[stage, 1, rows, :].astype(F32)
            if stage != 1:
                branch = 0.5 * branch
            value = (xg[stage, t, rows, :].astype(F32) + branch).astype(BF16)
            if stage < 2:
                xg[stage + 1, t, rows, :] = value
            else:
                result[rows, :] = value

        over(c * R, R, body)
        if stage < 2:
            gather_0(stage + 1, c)
        else:
            pltpu.make_async_copy(result.at[rows_of(c)], out.at[rows_of(c)], o_sem.at[c]).start()

    def mid(stage, c):
        if stage == 1:
            mixer(c)
        else:
            ffn(stage, c)

    tasks = dict(
        W=weights, G0=gather_0, G1=gather_1, G2=gather_2, G3=gather_3, N=norm, F=mid,
        DP=down_partner, DO=down_own, SA=sum_a, SB=sum_b, SC=sum_c,
    )
    for name, a, b in schedule():
        with jax.named_scope(f"{name}_{a}_{b}"):
            tasks[name](a, b)

    for c in range(NC):
        pltpu.make_async_copy(result.at[rows_of(c)], out.at[rows_of(c)], o_sem.at[c]).wait()
    for g, (first, count) in enumerate(GROUPS):
        await_bytes(w.at[pl.ds(0, 15), pl.ds(first, count)], w_send.at[g])
    for stage in range(3):
        for c in range(NC):
            await_bytes(xg.at[0, pl.ds(0, 7), rows_of(c)], y_send.at[stage, c])
            await_bytes(xg.at[0, pl.ds(0, 7), rows_of(c)], y_send.at[stage, c])


def on_device(
    tokens, first_gain, first_gate, first_up, first_down, mixer_gain, conv_input, outer_gate, inner_gate, conv_taps,
    mixer_out, second_gain, second_gate, second_up, second_down,
):
    shape = tokens.shape
    gains = jnp.stack([first_gain, mixer_gain, second_gain])
    hbm, vmem = pl.BlockSpec(memory_space=pl.ANY), pl.BlockSpec(memory_space=pltpu.VMEM)
    dma = pltpu.SemaphoreType.DMA
    result = pl.pallas_call(
        layer_kernel,
        out_shape=jax.ShapeDtypeStruct((ROWS, BLK), BF16),
        in_specs=[hbm, vmem, vmem] + [hbm] * 10,
        out_specs=hbm,
        scratch_shapes=[
            pltpu.VMEM((16, SLABS, 128, 128), BF16),
            pltpu.VMEM((3, 8, ROWS, BLK), BF16),
            pltpu.VMEM((ROWS, D), BF16),
            pltpu.VMEM((ROWS, 640), BF16),
            pltpu.VMEM((3, 4, ROWS, BLK), BF16),
            pltpu.VMEM((3, 4, ROWS, BLK), BF16),
            pltpu.VMEM((4, ROWS, BLK), F32),
            pltpu.VMEM((3, ROWS, BLK), BF16),
            pltpu.VMEM((3, ROWS, BLK), BF16),
            pltpu.VMEM((3, 2, ROWS, BLK), BF16),
            pltpu.VMEM((3, 2, ROWS, BLK), BF16),
            pltpu.VMEM((2, 8 + LEN, 128), F32),
            pltpu.VMEM((R, 128), F32),
            pltpu.VMEM((ROWS, 128), BF16),
            pltpu.VMEM((ROWS, BLK), BF16),
            dma((5,)),
            dma,
            dma((5,)),
            dma((5, 7)),
            dma((3, NC)),
            dma((3, NC, 3)),
            dma((3, NC, 3)),
            dma((NC,)),
        ],
        compiler_params=pltpu.CompilerParams(
            collective_id=0, has_side_effects=True, vmem_limit_bytes=67_000_000
        ),
    )(
        tokens.reshape(ROWS, BLK), gains, conv_taps, first_gate, first_up, first_down, conv_input, outer_gate,
        inner_gate, mixer_out, second_gate, second_up, second_down,
    )
    return result.reshape(shape)


def solution(mesh):
    fs, tp = P("fs", "tp"), P("tp", "fs")
    in_specs = (
        P("fs", None, "tp"), P(), fs, fs, tp, P(), fs, fs, fs, P(None, "tp"), tp, P(), fs, fs, tp,
    )
    return jax.shard_map(
        on_device, mesh=mesh, in_specs=in_specs, out_specs=P("fs", None, "tp"), check_vma=False
    )
```

time: 432 us -> 162 us (0.38)
  waiting for transfers between devices: 328 us -> 0 us
  Pallas kernels: 0 us -> 159 us
  matrix products: 42.9 us -> 0 us
  starting transfers between devices: 23 us -> 0 us
  other arithmetic: 17.8 us -> 1.37 us
  between operations: 13.4 us -> 0.01 us
  local copies, waits for them, and re-layouts: 6.23 us -> 1.77 us
    all_gather x6 -> x0, waiting for transfers between devices: 220 us -> none  [the longest x3 157 us: sent_together(): lax.all_gather(both, axis, axis=dim, tiled=True)]
    pallas_call x0 -> x1, Pallas kernels: none -> 159 us  [on_device(): pl.pallas_call(layer_kernel, out_shape=jax.ShapeDtypeStruct((ROWS, BLK),...]
    reduce_scatter x3 -> x0, waiting for transfers between devices: 107 us -> none  [project_down(): lax.psum_scatter(partial_sum.astype(jnp.bfloat16), 'tp', scatter_dimensio...]
    dot_general x7 -> x0, matrix products: 42.9 us -> none  [the longest x3 27.5 us: project_down(): jnp.dot(hidden, gathered_copies(weight, 'fs', 1), preferred_element_type=...]
    all_to_all x3 -> x0, starting transfers between devices: 22.3 us -> none  [copy_for_each(): return lax.all_to_all(copies, axis, split_axis=0, concat_axis=0, tiled=True)]
    reduce_sum x3 -> x0, other arithmetic: 8.16 us -> none  [norm_rows(): jnp.mean(values * values, axis=1, keepdims=True) + epsilon]
    convert_element_type x4 -> x0, other arithmetic: 6.35 us -> none  [the longest x2 3.72 us: half_ffn(): return (stream.astype(jnp.float32) + 0.5 * branch).astype(jnp.bfloat16)]
    broadcast_in_dim x3 -> x0, local copies, waits for them, and re-layouts: 4.72 us -> none  [copy_for_each(): copies = jnp.broadcast_to(value, (lax.axis_size(axis), *value.shape))]
  transfers between devices with their start and end apart: 12 -> 0, of which waited for: 9 -> 0; matrix products, arithmetic and copies ran while one was open for 8% -> 0% of each run, Pallas kernels for 0% -> 0%
where the time goes in v1:
time: 162 us
  Pallas kernels  159 us (98%)
  local copies, waits for them, and re-layouts  1.77 us (1%)
    pallas_call x1, Pallas kernels, on_device(): pl.pallas_call(layer_kernel, out_shape=jax.ShapeDtypeStruct((ROWS, BLK),...  159 us

profile of v1, /device:TPU:0, one launch (start us, length us, event | category | flops | bytes accessed | tf_op | source)
XLA Modules:
  0.0 161.7 jit_solution(14450953578064840518)
XLA Ops:
  0.0 1.4 pad_maximum_fusion.gains
  1.4 158.5 %shard_map.145 = bf16[768,256]{1,0:T(8,128)(2,1)} custom-call(bf16[768,256]{1,0:T(8,128)(2,1)} %bitcast.6, f32[3,2048]{1,0:T(4,128)} %pad_maximum_fusion.gains, f32[3,128]{1,0:T(4,128)} %taps.1, bf16[128,640]{1,0:T(8,128)(2,1)} %fgate.1, bf16[128,640]{1,0:T(8,128)(2,1)} %fup.1, bf16[640,128]{1,0:T(8,128)(2,1)} %fdown.1, bf16[128,128]{1,0:T(8,128)(2,1)} %conv_in.1, ...), custom_call_target="tpu_custom_call" | custom-call | tf_op jit(solution)/shard_map/pallas_call | solution.py:339
  159.9 1.8 %copy.17 = bf16[2,384,256]{2,1,0:T(8,128)(2,1)} copy(bf16[2,384,256]{2,1,0:T(8,128)(2,1)} %bitcast.5) | data formatting | bytes 786432

commit v2 on v1

--- a/solution.py
+++ b/solution.py
@@ -15,55 +15,63 @@
 ROWS = 768
 LEN = 384
 BLK = 256
-NC = 2
+NC = 4
 R = ROWS // NC
 HALF = R // 2
-SUB = 64
+SUB = 96
 SLABS = 34
 GROUPS = ((0, 10), (10, 5), (15, 4), (19, 10), (29, 5))
 UNITS = (0, 2, 3, 4, 3, 2, 1)
 AHEAD = (2, 1, 3, 0)
 
 
-def schedule():
-    order = [("W", 0, 0), ("G0", 0, 0), ("G0", 0, 1), ("W", 0, 1), ("G1", 0, 0), ("G1", 0, 1), ("W", 0, 2)]
-    order += [("G2", 0, 0), ("G2", 0, 1), ("G3", 0, 0), ("N", 0, 0), ("G3", 0, 1), ("N", 0, 1)]
-    order += [("W", 0, 3), ("W", 1, 0), ("W", 0, 4), ("W", 0, 5), ("W", 1, 1), ("F", 0, 0), ("W", 1, 2), ("F", 0, 1)]
-    order += [("W", 1, 3), ("W", 2, 0), ("W", 1, 4), ("W", 1, 5), ("W", 2, 1)]
-    order += [("DP", 0, 0), ("DO", 0, 0), ("SA", 0, 0), ("DP", 0, 1), ("DO", 0, 1), ("SA", 0, 1), ("W", 2, 2)]
-    order += [("SB", 0, 0), ("SB", 0, 1), ("W", 2, 3), ("W", 3, 0), ("SC", 0, 0), ("W", 2, 4), ("SC", 0, 1), ("W", 2, 5)]
-    order += [("G1", 1, 0), ("W", 3, 1), ("G2", 1, 0), ("G1", 1, 1), ("G3", 1, 0), ("N", 1, 0), ("F", 1, 0), ("DP", 1, 0)]
-    order += [("DO", 1, 0), ("SA", 1, 0), ("G2", 1, 1), ("G3", 1, 1), ("N", 1, 1), ("F", 1, 1), ("SB", 1, 0), ("DP", 1, 1)]
-    order += [("W", 3, 2), ("DO", 1, 1), ("SA", 1, 1), ("SC", 1, 0), ("SB", 1, 1), ("W", 3, 3), ("W", 4, 0), ("G1", 2, 0)]
-    order += [("SC", 1, 1), ("G2", 2, 0), ("W", 3, 4), ("G1", 2, 1), ("G3", 2, 0), ("N", 2, 0), ("G2", 2, 1), ("W", 3, 5)]
-    order += [("W", 4, 1), ("F", 2, 0), ("G3", 2, 1), ("N", 2, 1), ("F", 2, 1), ("W", 4, 2), ("W", 4, 3), ("W", 4, 4), ("W", 4, 5)]
-    order += [("DP", 2, 0), ("DO", 2, 0), ("SA", 2, 0), ("DP", 2, 1), ("DO", 2, 1), ("SA", 2, 1)]
-    order += [("SB", 2, 0), ("SB", 2, 1), ("SC", 2, 0), ("SC", 2, 1)]
-    return order
+ORDER = (
+    ("W", 0, 0), ("G0", 0, 1), ("W", 1, 0), ("W", 0, 1), ("G0", 0, 0), ("G0", 0, 2), ("G1", 0, 2), ("G1", 0, 1),
+    ("W", 0, 2), ("G2", 0, 1), ("G0", 0, 3), ("G1", 0, 0), ("G2", 0, 2), ("G1", 0, 3), ("W", 1, 1), ("W", 1, 2),
+    ("G3", 0, 2), ("G3", 0, 1), ("W", 0, 3), ("W", 0, 4), ("W", 1, 3), ("G2", 0, 0), ("W", 1, 4), ("W", 2, 0),
+    ("G2", 0, 3), ("G3", 0, 3), ("G3", 0, 0), ("N", 0, 0), ("N", 0, 2), ("N", 0, 3), ("W", 3, 0), ("N", 0, 1),
+    ("W", 0, 5), ("F", 0, 0), ("F", 0, 1), ("W", 1, 5), ("DA", 0, 1), ("DA", 0, 0), ("F", 0, 2), ("SA", 0, 1),
+    ("DA", 0, 2), ("DB", 0, 1), ("SA", 0, 0), ("W", 2, 1), ("DB", 0, 0), ("SA", 0, 2), ("SB", 0, 1), ("F", 0, 3),
+    ("DA", 0, 3), ("SB", 0, 0), ("DB", 0, 3), ("SA", 0, 3), ("W", 2, 2), ("SC", 0, 1), ("DB", 0, 2), ("W", 4, 0),
+    ("SC", 0, 0), ("SB", 0, 2), ("W", 2, 3), ("W", 2, 4), ("G1", 1, 0), ("G1", 1, 1), ("W", 3, 1), ("SB", 0, 3),
+    ("SC", 0, 2), ("G2", 1, 0), ("G2", 1, 1), ("W", 2, 5), ("W", 4, 1), ("G3", 1, 0), ("N", 1, 0), ("SC", 0, 3),
+    ("F", 1, 0), ("DA", 1, 0), ("G3", 1, 1), ("N", 1, 1), ("F", 1, 1), ("DA", 1, 1), ("G1", 1, 2), ("SA", 1, 0),
+    ("W", 3, 2), ("DB", 1, 0), ("DB", 1, 1), ("G1", 1, 3), ("G2", 1, 2), ("SA", 1, 1), ("SB", 1, 0), ("G2", 1, 3),
+    ("G3", 1, 2), ("N", 1, 2), ("SB", 1, 1), ("W", 4, 2), ("W", 3, 3), ("F", 1, 2), ("DA", 1, 2), ("G3", 1, 3),
+    ("SC", 1, 0), ("N", 1, 3), ("F", 1, 3), ("DA", 1, 3), ("SA", 1, 2), ("SC", 1, 1), ("DB", 1, 2), ("SA", 1, 3),
+    ("G1", 2, 0), ("SB", 1, 2), ("W", 3, 4), ("W", 4, 3), ("DB", 1, 3), ("W", 4, 4), ("G1", 2, 1), ("SB", 1, 3),
+    ("G2", 2, 0), ("G3", 2, 0), ("SC", 1, 2), ("G2", 2, 1), ("N", 2, 0), ("W", 3, 5), ("F", 2, 0), ("SC", 1, 3),
+    ("G3", 2, 1), ("N", 2, 1), ("W", 4, 5), ("DA", 2, 0), ("DB", 2, 0), ("G1", 2, 2), ("F", 2, 1), ("SA", 2, 0),
+    ("DA", 2, 1), ("G1", 2, 3), ("G2", 2, 2), ("DB", 2, 1), ("SA", 2, 1), ("SB", 2, 0), ("G3", 2, 2), ("G2", 2, 3),
+    ("N", 2, 2), ("F", 2, 2), ("DA", 2, 2), ("SB", 2, 1), ("G3", 2, 3), ("N", 2, 3), ("F", 2, 3), ("DA", 2, 3),
+    ("SA", 2, 2), ("DB", 2, 2), ("DB", 2, 3), ("SA", 2, 3), ("SB", 2, 2), ("SC", 2, 0), ("SB", 2, 3), ("SC", 2, 1),
+    ("SC", 2, 2), ("SC", 2, 3),
+)
 
 
 def layer_kernel(
-    tokens, gains, taps, fgate, fup, fdown, conv_in, outer_gate, inner_gate, mix_out, sgate, sup, sdown,
+    tokens, gain_1, gain_2, gain_3, taps_in, fgate, fup, fdown, conv_in, outer_gate, inner_gate, mix_out, sgate, sup, sdown,
     out,
-    w, xg, normed, hidden, psend, precv, pown, s1, r1, s2, r2, gi, outer_s, mixed, result,
-    w_load, x_load, w_send, w_recv, y_send, g_recv, s_recv, o_sem,
+    w, xg, normed, hidden, psend, precv, pown, s1, r1, s2, r2, gi, outer_s, mixed, result, gains, taps,
+    w_load, x_load, w_send, w_recv, y_send, g_recv, s_recv, o_sem, k_load,
 ):
     f, t = lax.axis_index("fs"), lax.axis_index("tp")
-    z, x = f // 4, f % 4
-    y, core = t // 2, t % 2
+    z, x = lax.div(f, 4), lax.rem(f, 4)
+    y, core = lax.div(t, 2), lax.rem(t, 2)
     other = 1 - core
+    zs = [4 * lax.rem(z + i, 4) for i in range(4)]
+    xs = [lax.rem(x + i, 4) for i in range(4)]
+    ys = [2 * lax.rem(y + i, 4) for i in range(4)]
+    slots = [[zs[i] + xs[j] for j in range(4)] for i in range(4)]
+    mine, others = [a + core for a in ys], [a + other for a in ys]
 
     def slot(h, a, b):
-        za, xa = (b, a) if h == 0 else (a, b)
-        return ((z + za) % 4) * 4 + (x + xa) % 4
-
-    def at_y(ahead, which):
-        return ((y + ahead) % 4) * 2 + which
+        return slots[b][a] if h == 0 else slots[a][b]
 
     def w_device(h, phase, d):
         return (slot(h, d, 0) if phase == 1 else slot(h, 0, d), t)
 
-    up, down, partner = (f, at_y(1, core)), (f, at_y(3, core)), (f, at_y(0, other))
+    above, below, partner = (f, mine[1]), (f, mine[3]), (f, others[0])
 
     def load_tokens():
         return pltpu.make_async_copy(tokens, xg.at[0, t], x_load)
@@ -85,19 +93,27 @@
     def await_bytes(ref, sem):
         pltpu.make_async_copy(ref, ref, sem).wait()
 
+    def load_vectors():
+        copies = [pltpu.make_async_copy(a, gains.at[i], k_load.at[i]) for i, a in enumerate((gain_1, gain_2, gain_3))]
+        return copies + [pltpu.make_async_copy(taps_in, taps, k_load.at[3])]
+
     load_tokens().start()
     for g in range(5):
         for copy in loads(g):
             copy.start()
+    for copy in load_vectors():
+        copy.start()
 
     barrier = pltpu.get_barrier_semaphore()
-    peers = [w_device(h, 1, d) for h in (0, 1) for d in (1, 3)] + [up, down, partner]
+    peers = [w_device(h, 1, d) for h in (0, 1) for d in (1, 3)] + [above, below, partner]
     for peer in peers:
         pl.semaphore_signal(barrier, inc=1, device_id=peer, device_id_type=MESH)
 
     gi[:, pl.ds(0, 8), :] = jnp.zeros((2, 8, 128), F32)
 
     load_tokens().wait()
+    for copy in load_vectors():
+        copy.wait()
     pl.semaphore_wait(barrier, len(peers))
 
     def w_copy(g, h, a, b, phase, d, quarter, landing):
@@ -135,16 +151,19 @@
                 back = 4 - d
                 if rnd == 1:
                     w_copy(g, h, back, 0, 1, d, True, 2)
-                    w_copy(g, h, 1, 0, 2, d, False, 3)
-                    w_copy(g, h, 3, 0, 2, d, False, 3)
                 elif rnd == 2:
                     w_copy(g, h, 0, back, 2, d, True, 4)
-                    w_copy(g, h, 2, 0, 2, d, False, 4)
                 elif rnd == 3:
                     w_copy(g, h, 1, back, 2, d, True, 5)
                     w_copy(g, h, 3, back, 2, d, True, 5)
                 else:
                     w_copy(g, h, 2, back, 2, d, True, 6)
+            for h, d in both:
+                if rnd == 1:
+                    w_copy(g, h, 1, 0, 2, d, False, 3)
+                    w_copy(g, h, 3, 0, 2, d, False, 3)
+                elif rnd == 2:
+                    w_copy(g, h, 2, 0, 2, d, False, 4)
 
     def y_copy(src, dst, stage, c, recv, device):
         pltpu.make_async_remote_copy(
@@ -162,24 +181,24 @@
         return pl.ds(c * R + HALF, HALF)
 
     def gather_0(stage, c):
-        mine = xg.at[stage, t, rows_of(c)]
-        for device in (up, down):
-            y_copy(mine, mine, stage, c, g_recv.at[stage, c, 0], device)
-        y_copy(mine, mine, stage, c, g_recv.at[stage, c, 2], partner)
+        ref = xg.at[stage, t, rows_of(c)]
+        for device in (above, below):
+            y_copy(ref, ref, stage, c, g_recv.at[stage, c, 0], device)
+        y_copy(ref, ref, stage, c, g_recv.at[stage, c, 2], partner)
 
     def gather_1(stage, c):
         await_bytes(xg.at[stage, pl.ds(0, 2), rows_of(c)], g_recv.at[stage, c, 0])
-        below, above = at_y(3, core), at_y(1, core)
-        for block, part, device in ((below, front(c), up), (above, rear(c), down)):
+        blocks = mine[3], mine[1]
+        for block, part, device in ((blocks[0], front(c), above), (blocks[1], rear(c), below)):
             ref = xg.at[stage, block, part]
             y_copy(ref, ref, stage, c, g_recv.at[stage, c, 1], device)
-        for block in (below, above):
+        for block in blocks:
             ref = xg.at[stage, block, rows_of(c)]
             y_copy(ref, ref, stage, c, g_recv.at[stage, c, 2], partner)
 
     def gather_2(stage, c):
         await_bytes(xg.at[stage, 0, rows_of(c)], g_recv.at[stage, c, 1])
-        ref = xg.at[stage, at_y(2, core), rows_of(c)]
+        ref = xg.at[stage, mine[2], rows_of(c)]
         y_copy(ref, ref, stage, c, g_recv.at[stage, c, 2], partner)
 
     def gather_3(stage, c):
@@ -198,7 +217,7 @@
             for b in range(8):
                 v = xg[stage, b, rows, :].astype(F32)
                 cols = pl.ds(b * BLK, BLK)
-                normed[rows, cols] = (v * scale * gains[stage : stage + 1, cols]).astype(BF16)
+                normed[rows, cols] = (v * scale * gains[stage, :, cols]).astype(BF16)
 
     def columns(first):
         return w[:, first].reshape(D, 128)
@@ -206,13 +225,10 @@
     def ffn(stage, c):
         first = 0 if stage == 0 else 19
 
-        @pl.loop(0, 5)
-        def _(s):
-            pair = jnp.concatenate([columns(first + 2 * s), columns(first + 2 * s + 1)], axis=1)
-            both_halves = jnp.dot(normed[rows_of(c), :], pair, preferred_element_type=F32)
-            gate, upward = both_halves[:, :128], both_halves[:, 128:]
-            value = gate / (1.0 + jnp.exp(-gate)) * upward
-            hidden[rows_of(c), pl.ds(pl.multiple_of(128 * s, 128), 128)] = value.astype(BF16)
+        all_columns = jnp.concatenate([columns(first + 2 * s + i) for i in (0, 1) for s in range(5)], axis=1)
+        products = jnp.dot(normed[rows_of(c), :], all_columns, preferred_element_type=F32)
+        gate, upward = products[:, :640], products[:, 640:]
+        hidden[rows_of(c), :] = (gate / (1.0 + jnp.exp(-gate)) * upward).astype(BF16)
 
     def mixer(c):
         three = jnp.concatenate([columns(15), columns(16), columns(17)], axis=1)
@@ -225,44 +241,48 @@
         convolved = convolved + taps[2:3, :] * gi[seq, pl.ds(8 + at, R), :]
         mixed[rows_of(c), :] = (outer_s[...] * convolved).astype(BF16)
 
-    def product(stage, c, block):
-        a, b = 2 * block, 2 * block + 1
+    def product(stage, c, blocks):
         if stage == 1:
-            pair = jnp.concatenate([w[a, 18], w[b, 18]], axis=1)
-            return jnp.dot(mixed[rows_of(c), :], pair, preferred_element_type=F32)
-        slabs = pl.ds(10 if stage == 0 else 29, 5)
-        pair = jnp.concatenate([w[a, slabs].reshape(640, 128), w[b, slabs].reshape(640, 128)], axis=1)
-        return jnp.dot(hidden[rows_of(c), :], pair, preferred_element_type=F32)
-
-    def down_partner(stage, c):
-        for i in range(4):
-            psend[stage, i, rows_of(c), :] = product(stage, c, at_y(AHEAD[i], other)).astype(BF16)
-        part = pl.ds(0, 4)
-        y_copy(psend.at[stage, part, rows_of(c)], precv.at[stage, part, rows_of(c)], stage, c, s_recv.at[stage, c, 0], partner)
-
-    def down_own(stage, c):
-        for i in range(4):
-            pown[i, rows_of(c), :] = product(stage, c, at_y(AHEAD[i], core))
+            rows, columns = mixed[rows_of(c), :], [w[2 * b + i, 18] for b in blocks for i in (0, 1)]
+        else:
+            slabs = pl.ds(10 if stage == 0 else 29, 5)
+            rows, columns = hidden[rows_of(c), :], [w[2 * b + i, slabs].reshape(640, 128) for b in blocks for i in (0, 1)]
+        return jnp.dot(rows, jnp.concatenate(columns, axis=1), preferred_element_type=F32)
+
+    def down(stage, c, first, count, landing):
+        products = product(stage, c, [others[AHEAD[i]] for i in range(first, first + count)])
+        for i in range(count):
+            psend[stage, first + i, rows_of(c), :] = products[:, BLK * i : BLK * (i + 1)].astype(BF16)
+        part = pl.ds(first, count)
+        y_copy(psend.at[stage, part, rows_of(c)], precv.at[stage, part, rows_of(c)], stage, c, s_recv.at[stage, c, landing], partner)
+        products = product(stage, c, [mine[AHEAD[i]] for i in range(first, first + count)])
+        for i in range(count):
+            pown[first + i, rows_of(c), :] = products[:, BLK * i : BLK * (i + 1)]
+
+    def down_first(stage, c):
+        down(stage, c, 0, 1, 0)
+
+    def down_rest(stage, c):
+        down(stage, c, 1, 3, 3)
 
     def pair_sum(stage, i, rows):
         return pown[i, rows, :] + precv[stage, i, rows, :].astype(F32)
 
     def over(first, count, body):
-        @pl.loop(0, count // SUB)
-        def _(i):
-            body(pl.ds(pl.multiple_of(first + i * SUB, SUB), SUB))
+        body(pl.ds(first, count))
 
     def sum_a(stage, c):
-        await_bytes(precv.at[stage, pl.ds(0, 4), rows_of(c)], s_recv.at[stage, c, 0])
+        await_bytes(precv.at[stage, 0, rows_of(c)], s_recv.at[stage, c, 0])
 
         def body(rows):
             s1[stage, rows, :] = pair_sum(stage, 0, rows).astype(BF16)
 
         over(c * R, R, body)
-        for part, device in ((front(c), up), (rear(c), down)):
+        for part, device in ((front(c), above), (rear(c), below)):
             y_copy(s1.at[stage, part], r1.at[stage, part], stage, c, s_recv.at[stage, c, 1], device)
 
     def sum_b(stage, c):
+        await_bytes(precv.at[stage, pl.ds(1, 3), rows_of(c)], s_recv.at[stage, c, 3])
         await_bytes(r1.at[stage, rows_of(c)], s_recv.at[stage, c, 1])
 
         def with_r1(i, rows):
@@ -282,7 +302,7 @@
 
         over(c * R, HALF, front_body)
         over(c * R + HALF, HALF, rear_body)
-        for i, device in ((0, up), (1, down)):
+        for i, device in ((0, above), (1, below)):
             y_copy(s2.at[stage, i, rows_of(c)], r2.at[stage, i, rows_of(c)], stage, c, s_recv.at[stage, c, 2], device)
 
     def sum_c(stage, c):
@@ -312,9 +332,9 @@
 
     tasks = dict(
         W=weights, G0=gather_0, G1=gather_1, G2=gather_2, G3=gather_3, N=norm, F=mid,
-        DP=down_partner, DO=down_own, SA=sum_a, SB=sum_b, SC=sum_c,
+        DA=down_first, DB=down_rest, SA=sum_a, SB=sum_b, SC=sum_c,
     )
-    for name, a, b in schedule():
+    for name, a, b in ORDER:
         with jax.named_scope(f"{name}_{a}_{b}"):
             tasks[name](a, b)
 
@@ -333,13 +353,12 @@
     mixer_out, second_gain, second_gate, second_up, second_down,
 ):
     shape = tokens.shape
-    gains = jnp.stack([first_gain, mixer_gain, second_gain])
-    hbm, vmem = pl.BlockSpec(memory_space=pl.ANY), pl.BlockSpec(memory_space=pltpu.VMEM)
+    hbm = pl.BlockSpec(memory_space=pl.ANY)
     dma = pltpu.SemaphoreType.DMA
     result = pl.pallas_call(
         layer_kernel,
         out_shape=jax.ShapeDtypeStruct((ROWS, BLK), BF16),
-        in_specs=[hbm, vmem, vmem] + [hbm] * 10,
+        in_specs=[hbm] * 15,
         out_specs=hbm,
         scratch_shapes=[
             pltpu.VMEM((16, SLABS, 128, 128), BF16),
@@ -357,20 +376,23 @@
             pltpu.VMEM((R, 128), F32),
             pltpu.VMEM((ROWS, 128), BF16),
             pltpu.VMEM((ROWS, BLK), BF16),
+            pltpu.VMEM((3, 1, D), F32),
+            pltpu.VMEM((3, 128), F32),
             dma((5,)),
             dma,
             dma((5,)),
             dma((5, 7)),
             dma((3, NC)),
             dma((3, NC, 3)),
-            dma((3, NC, 3)),
+            dma((3, NC, 4)),
             dma((NC,)),
+            dma((4,)),
         ],
         compiler_params=pltpu.CompilerParams(
             collective_id=0, has_side_effects=True, vmem_limit_bytes=67_000_000
         ),
     )(
-        tokens.reshape(ROWS, BLK), gains, conv_taps, first_gate, first_up, first_down, conv_input, outer_gate,
+        tokens.reshape(ROWS, BLK), first_gain[None], mixer_gain[None], second_gain[None], conv_taps, first_gate, first_up, first_down, conv_input, outer_gate,
         inner_gate, mixer_out, second_gate, second_up, second_down,
     )
     return result.reshape(shape)

time: 162 us -> 128 us (0.79)
  Pallas kernels: 159 us -> 126 us
    pallas_call x1, Pallas kernels: 159 us -> 126 us  [on_device(): pl.pallas_call(layer_kernel, out_shape=jax.ShapeDtypeStruct((ROWS, BLK),...]
where the time goes in v2:
time: 128 us
  Pallas kernels  126 us (98%)
  local copies, waits for them, and re-layouts  1.77 us (1%)
    pallas_call x1, Pallas kernels, on_device(): pl.pallas_call(layer_kernel, out_shape=jax.ShapeDtypeStruct((ROWS, BLK),...  126 us

profile of v2, /device:TPU:0, one launch (start us, length us, event | category | flops | bytes accessed | tf_op | source)
XLA Modules:
  0.0 128.2 jit_solution(8115582246204890496)
XLA Ops:
  0.0 126.4 %shard_map.145 = bf16[768,256]{1,0:T(8,128)(2,1)} custom-call(bf16[768,256]{1,0:T(8,128)(2,1)} %bitcast.6, f32[1,2048]{1,0:T(1,128)} %bitcast.7, f32[1,2048]{1,0:T(1,128)} %bitcast.8, f32[1,2048]{1,0:T(1,128)} %bitcast.9, f32[3,128]{1,0:T(4,128)} %taps_in.1, bf16[128,640]{1,0:T(8,128)(2,1)} %fgate.1, bf16[128,640]{1,0:T(8,128)(2,1)} %fup.1, ...), custom_call_target="tpu_custom_call" | custom-call | tf_op jit(solution)/shard_map/pallas_call | solution.py:358
  126.4 1.8 %copy.17 = bf16[2,384,256]{2,1,0:T(8,128)(2,1)} copy(bf16[2,384,256]{2,1,0:T(8,128)(2,1)} %bitcast.5) | data formatting | bytes 786432

commit v3 on v2

--- a/solution.py
+++ b/solution.py
@@ -26,34 +26,37 @@
 
 
 ORDER = (
-    ("W", 0, 0), ("G0", 0, 1), ("W", 1, 0), ("W", 0, 1), ("G0", 0, 0), ("G0", 0, 2), ("G1", 0, 2), ("G1", 0, 1),
-    ("W", 0, 2), ("G2", 0, 1), ("G0", 0, 3), ("G1", 0, 0), ("G2", 0, 2), ("G1", 0, 3), ("W", 1, 1), ("W", 1, 2),
-    ("G3", 0, 2), ("G3", 0, 1), ("W", 0, 3), ("W", 0, 4), ("W", 1, 3), ("G2", 0, 0), ("W", 1, 4), ("W", 2, 0),
-    ("G2", 0, 3), ("G3", 0, 3), ("G3", 0, 0), ("N", 0, 0), ("N", 0, 2), ("N", 0, 3), ("W", 3, 0), ("N", 0, 1),
-    ("W", 0, 5), ("F", 0, 0), ("F", 0, 1), ("W", 1, 5), ("DA", 0, 1), ("DA", 0, 0), ("F", 0, 2), ("SA", 0, 1),
-    ("DA", 0, 2), ("DB", 0, 1), ("SA", 0, 0), ("W", 2, 1), ("DB", 0, 0), ("SA", 0, 2), ("SB", 0, 1), ("F", 0, 3),
-    ("DA", 0, 3), ("SB", 0, 0), ("DB", 0, 3), ("SA", 0, 3), ("W", 2, 2), ("SC", 0, 1), ("DB", 0, 2), ("W", 4, 0),
-    ("SC", 0, 0), ("SB", 0, 2), ("W", 2, 3), ("W", 2, 4), ("G1", 1, 0), ("G1", 1, 1), ("W", 3, 1), ("SB", 0, 3),
-    ("SC", 0, 2), ("G2", 1, 0), ("G2", 1, 1), ("W", 2, 5), ("W", 4, 1), ("G3", 1, 0), ("N", 1, 0), ("SC", 0, 3),
-    ("F", 1, 0), ("DA", 1, 0), ("G3", 1, 1), ("N", 1, 1), ("F", 1, 1), ("DA", 1, 1), ("G1", 1, 2), ("SA", 1, 0),
-    ("W", 3, 2), ("DB", 1, 0), ("DB", 1, 1), ("G1", 1, 3), ("G2", 1, 2), ("SA", 1, 1), ("SB", 1, 0), ("G2", 1, 3),
-    ("G3", 1, 2), ("N", 1, 2), ("SB", 1, 1), ("W", 4, 2), ("W", 3, 3), ("F", 1, 2), ("DA", 1, 2), ("G3", 1, 3),
-    ("SC", 1, 0), ("N", 1, 3), ("F", 1, 3), ("DA", 1, 3), ("SA", 1, 2), ("SC", 1, 1), ("DB", 1, 2), ("SA", 1, 3),
-    ("G1", 2, 0), ("SB", 1, 2), ("W", 3, 4), ("W", 4, 3), ("DB", 1, 3), ("W", 4, 4), ("G1", 2, 1), ("SB", 1, 3),
-    ("G2", 2, 0), ("G3", 2, 0), ("SC", 1, 2), ("G2", 2, 1), ("N", 2, 0), ("W", 3, 5), ("F", 2, 0), ("SC", 1, 3),
-    ("G3", 2, 1), ("N", 2, 1), ("W", 4, 5), ("DA", 2, 0), ("DB", 2, 0), ("G1", 2, 2), ("F", 2, 1), ("SA", 2, 0),
-    ("DA", 2, 1), ("G1", 2, 3), ("G2", 2, 2), ("DB", 2, 1), ("SA", 2, 1), ("SB", 2, 0), ("G3", 2, 2), ("G2", 2, 3),
-    ("N", 2, 2), ("F", 2, 2), ("DA", 2, 2), ("SB", 2, 1), ("G3", 2, 3), ("N", 2, 3), ("F", 2, 3), ("DA", 2, 3),
-    ("SA", 2, 2), ("DB", 2, 2), ("DB", 2, 3), ("SA", 2, 3), ("SB", 2, 2), ("SC", 2, 0), ("SB", 2, 3), ("SC", 2, 1),
-    ("SC", 2, 2), ("SC", 2, 3),
+    ("W", 0, 0), ("G0", 0, 2), ("G0", 0, 3), ("G1", 0, 2), ("G0", 0, 0), ("W", 0, 1), ("G1", 0, 0), ("GH", 0, 0),
+    ("G1", 0, 3), ("W", 1, 0), ("W", 0, 2), ("G0", 0, 1), ("W", 0, 3), ("G1", 0, 1), ("GH", 0, 1), ("W", 1, 1),
+    ("GH", 0, 2), ("G2", 0, 2), ("G3", 0, 2), ("G2", 0, 1), ("GH", 0, 3), ("G2", 0, 0), ("N", 0, 2), ("G2", 0, 3),
+    ("G3", 0, 3), ("N", 0, 3), ("G3", 0, 0), ("N", 0, 0), ("W", 1, 2), ("W", 0, 4), ("G3", 0, 1), ("W", 1, 3),
+    ("N", 0, 1), ("W", 1, 4), ("W", 2, 0), ("W", 3, 0), ("W", 0, 5), ("F", 0, 3), ("F", 0, 0), ("W", 1, 5),
+    ("DA", 0, 0), ("DA", 0, 3), ("DB", 0, 3), ("DB", 0, 0), ("SA", 0, 0), ("SA", 0, 3), ("F", 0, 2), ("DA", 0, 2),
+    ("SE", 0, 0), ("DB", 0, 2), ("W", 2, 1), ("SB", 0, 0), ("SE", 0, 3), ("SA", 0, 2), ("F", 0, 1), ("SE", 0, 2),
+    ("W", 2, 2), ("SC", 0, 0), ("DA", 0, 1), ("SB", 0, 2), ("SB", 0, 3), ("W", 4, 0), ("G1", 1, 0), ("DB", 0, 1),
+    ("W", 2, 3), ("SA", 0, 1), ("W", 2, 4), ("SC", 0, 2), ("W", 3, 1), ("SC", 0, 3), ("GH", 1, 0), ("G2", 1, 0),
+    ("G1", 1, 2), ("SE", 0, 1), ("W", 2, 5), ("SB", 0, 1), ("G3", 1, 0), ("N", 1, 0), ("W", 4, 1), ("GH", 1, 2),
+    ("F", 1, 0), ("DA", 1, 0), ("DB", 1, 0), ("G1", 1, 3), ("G2", 1, 2), ("SA", 1, 0), ("SC", 0, 1), ("GH", 1, 3),
+    ("G2", 1, 3), ("G3", 1, 2), ("N", 1, 2), ("F", 1, 2), ("SE", 1, 0), ("DA", 1, 2), ("SB", 1, 0), ("DB", 1, 2),
+    ("W", 3, 2), ("G3", 1, 3), ("N", 1, 3), ("G1", 1, 1), ("F", 1, 3), ("DA", 1, 3), ("W", 3, 3), ("SA", 1, 2),
+    ("SE", 1, 2), ("DB", 1, 3), ("GH", 1, 1), ("SA", 1, 3), ("G2", 1, 1), ("SC", 1, 0), ("SE", 1, 3), ("W", 4, 2),
+    ("G3", 1, 1), ("N", 1, 1), ("F", 1, 1), ("SB", 1, 3), ("DA", 1, 1), ("SB", 1, 2), ("G1", 2, 0), ("GH", 2, 0),
+    ("DB", 1, 1), ("W", 3, 4), ("W", 4, 3), ("SA", 1, 1), ("SC", 1, 3), ("G2", 2, 0), ("SE", 1, 1), ("SB", 1, 1),
+    ("W", 4, 4), ("G1", 2, 3), ("GH", 2, 3), ("G3", 2, 0), ("SC", 1, 2), ("N", 2, 0), ("W", 3, 5), ("F", 2, 0),
+    ("SC", 1, 1), ("G2", 2, 3), ("G1", 2, 2), ("W", 4, 5), ("DA", 2, 0), ("DB", 2, 0), ("GH", 2, 2), ("G3", 2, 3),
+    ("N", 2, 3), ("G1", 2, 1), ("F", 2, 3), ("DA", 2, 3), ("G2", 2, 2), ("GH", 2, 1), ("SA", 2, 0), ("SE", 2, 0),
+    ("DB", 2, 3), ("G2", 2, 1), ("SA", 2, 3), ("G3", 2, 2), ("N", 2, 2), ("F", 2, 2), ("DA", 2, 2), ("SB", 2, 0),
+    ("SE", 2, 3), ("G3", 2, 1), ("N", 2, 1), ("F", 2, 1), ("DA", 2, 1), ("SA", 2, 2), ("DB", 2, 2), ("SB", 2, 3),
+    ("DB", 2, 1), ("SC", 2, 0), ("SA", 2, 1), ("SE", 2, 2), ("SB", 2, 2), ("SE", 2, 1), ("SC", 2, 3), ("SB", 2, 1),
+    ("SC", 2, 2), ("SC", 2, 1),
 )
 
 
 def layer_kernel(
     tokens, gain_1, gain_2, gain_3, taps_in, fgate, fup, fdown, conv_in, outer_gate, inner_gate, mix_out, sgate, sup, sdown,
     out,
-    w, xg, normed, hidden, psend, precv, pown, s1, r1, s2, r2, gi, outer_s, mixed, result, gains, taps,
-    w_load, x_load, w_send, w_recv, y_send, g_recv, s_recv, o_sem, k_load,
+    w, xg, normed, hidden, psend, precv, pown, s1, r1, s2, r2, gi, outer_s, mixed, gains, taps,
+    w_load, x_load, w_send, w_recv, y_send, g_recv, s_recv, k_load,
 ):
     f, t = lax.axis_index("fs"), lax.axis_index("tp")
     z, x = lax.div(f, 4), lax.rem(f, 4)
@@ -182,17 +185,21 @@
 
     def gather_0(stage, c):
         ref = xg.at[stage, t, rows_of(c)]
-        for device in (above, below):
-            y_copy(ref, ref, stage, c, g_recv.at[stage, c, 0], device)
+        for landing, parts in ((0, (front(c), rear(c))), (3, (rear(c), front(c)))):
+            for part, device in zip(parts, (above, below)):
+                half = xg.at[stage, t, part]
+                y_copy(half, half, stage, c, g_recv.at[stage, c, landing], device)
         y_copy(ref, ref, stage, c, g_recv.at[stage, c, 2], partner)
 
     def gather_1(stage, c):
-        await_bytes(xg.at[stage, pl.ds(0, 2), rows_of(c)], g_recv.at[stage, c, 0])
-        blocks = mine[3], mine[1]
-        for block, part, device in ((blocks[0], front(c), above), (blocks[1], rear(c), below)):
+        await_bytes(xg.at[stage, 0, rows_of(c)], g_recv.at[stage, c, 0])
+        for block, part, device in ((mine[3], front(c), above), (mine[1], rear(c), below)):
             ref = xg.at[stage, block, part]
             y_copy(ref, ref, stage, c, g_recv.at[stage, c, 1], device)
-        for block in blocks:
+
+    def gather_rest(stage, c):
+        await_bytes(xg.at[stage, 0, rows_of(c)], g_recv.at[stage, c, 3])
+        for block in (mine[3], mine[1]):
             ref = xg.at[stage, block, rows_of(c)]
             y_copy(ref, ref, stage, c, g_recv.at[stage, c, 2], partner)
 
@@ -268,61 +275,41 @@
     def pair_sum(stage, i, rows):
         return pown[i, rows, :] + precv[stage, i, rows, :].astype(F32)
 
-    def over(first, count, body):
-        body(pl.ds(first, count))
-
     def sum_a(stage, c):
         await_bytes(precv.at[stage, 0, rows_of(c)], s_recv.at[stage, c, 0])
-
-        def body(rows):
-            s1[stage, rows, :] = pair_sum(stage, 0, rows).astype(BF16)
-
-        over(c * R, R, body)
+        s1[stage, rows_of(c), :] = pair_sum(stage, 0, rows_of(c)).astype(BF16)
         for part, device in ((front(c), above), (rear(c), below)):
             y_copy(s1.at[stage, part], r1.at[stage, part], stage, c, s_recv.at[stage, c, 1], device)
 
+    def send_halves(stage, c, parts, with_r1):
+        for i, part, device in ((1, parts[0], above), (2, parts[1], below)):
+            value = pair_sum(stage, i, part)
+            if with_r1:
+                value = value + r1[stage, part, :].astype(F32)
+            s2[stage, i - 1, part, :] = value.astype(BF16)
+            y_copy(s2.at[stage, i - 1, part], r2.at[stage, i - 1, part], stage, c, s_recv.at[stage, c, 2], device)
+
+    def sum_early(stage, c):
+        await_bytes(precv.at[stage, pl.ds(1, 3), rows_of(c)], s_recv.at[stage, c, 3])
+        send_halves(stage, c, (rear(c), front(c)), False)
+
     def sum_b(stage, c):
-        await_bytes(precv.at[stage, pl.ds(1, 3), rows_of(c)], s_recv.at[stage, c, 3])
         await_bytes(r1.at[stage, rows_of(c)], s_recv.at[stage, c, 1])
-
-        def with_r1(i, rows):
-            value = pair_sum(stage, i, rows) + r1[stage, rows, :].astype(F32)
-            s2[stage, i - 1, rows, :] = value.astype(BF16)
-
-        def alone(i, rows):
-            s2[stage, i - 1, rows, :] = pair_sum(stage, i, rows).astype(BF16)
-
-        def front_body(rows):
-            with_r1(1, rows)
-            alone(2, rows)
-
-        def rear_body(rows):
-            alone(1, rows)
-            with_r1(2, rows)
-
-        over(c * R, HALF, front_body)
-        over(c * R + HALF, HALF, rear_body)
-        for i, device in ((0, above), (1, below)):
-            y_copy(s2.at[stage, i, rows_of(c)], r2.at[stage, i, rows_of(c)], stage, c, s_recv.at[stage, c, 2], device)
+        send_halves(stage, c, (front(c), rear(c)), True)
 
     def sum_c(stage, c):
         await_bytes(r2.at[stage, pl.ds(0, 2), rows_of(c)], s_recv.at[stage, c, 2])
 
-        def body(rows):
-            branch = pair_sum(stage, 3, rows) + r2[stage, 0, rows, :].astype(F32) + r2[stage, 1, rows, :].astype(F32)
-            if stage != 1:
-                branch = 0.5 * branch
-            value = (xg[stage, t, rows, :].astype(F32) + branch).astype(BF16)
-            if stage < 2:
-                xg[stage + 1, t, rows, :] = value
-            else:
-                result[rows, :] = value
-
-        over(c * R, R, body)
+        rows = rows_of(c)
+        branch = pair_sum(stage, 3, rows) + r2[stage, 0, rows, :].astype(F32) + r2[stage, 1, rows, :].astype(F32)
+        if stage != 1:
+            branch = 0.5 * branch
+        value = (xg[stage, t, rows, :].astype(F32) + branch).astype(BF16)
         if stage < 2:
+            xg[stage + 1, t, rows, :] = value
             gather_0(stage + 1, c)
         else:
-            pltpu.make_async_copy(result.at[rows_of(c)], out.at[rows_of(c)], o_sem.at[c]).start()
+            out[rows, :] = value
 
     def mid(stage, c):
         if stage == 1:
@@ -331,15 +318,13 @@
             ffn(stage, c)
 
     tasks = dict(
-        W=weights, G0=gather_0, G1=gather_1, G2=gather_2, G3=gather_3, N=norm, F=mid,
-        DA=down_first, DB=down_rest, SA=sum_a, SB=sum_b, SC=sum_c,
+        W=weights, G0=gather_0, G1=gather_1, GH=gather_rest, G2=gather_2, G3=gather_3, N=norm, F=mid,
+        DA=down_first, DB=down_rest, SA=sum_a, SE=sum_early, SB=sum_b, SC=sum_c,
     )
     for name, a, b in ORDER:
         with jax.named_scope(f"{name}_{a}_{b}"):
             tasks[name](a, b)
 
-    for c in range(NC):
-        pltpu.make_async_copy(result.at[rows_of(c)], out.at[rows_of(c)], o_sem.at[c]).wait()
     for g, (first, count) in enumerate(GROUPS):
         await_bytes(w.at[pl.ds(0, 15), pl.ds(first, count)], w_send.at[g])
     for stage in range(3):
@@ -357,9 +342,9 @@
     dma = pltpu.SemaphoreType.DMA
     result = pl.pallas_call(
         layer_kernel,
-        out_shape=jax.ShapeDtypeStruct((ROWS, BLK), BF16),
+        out_shape=pltpu.VMEM((ROWS, BLK), BF16),
         in_specs=[hbm] * 15,
-        out_specs=hbm,
+        out_specs=pl.BlockSpec(memory_space=pltpu.VMEM),
         scratch_shapes=[
             pltpu.VMEM((16, SLABS, 128, 128), BF16),
             pltpu.VMEM((3, 8, ROWS, BLK), BF16),
@@ -375,7 +360,6 @@
             pltpu.VMEM((2, 8 + LEN, 128), F32),
             pltpu.VMEM((R, 128), F32),
             pltpu.VMEM((ROWS, 128), BF16),
-            pltpu.VMEM((ROWS, BLK), BF16),
             pltpu.VMEM((3, 1, D), F32),
             pltpu.VMEM((3, 128), F32),
             dma((5,)),
@@ -383,13 +367,12 @@
             dma((5,)),
             dma((5, 7)),
             dma((3, NC)),
-            dma((3, NC, 3)),
             dma((3, NC, 4)),
-            dma((NC,)),
+            dma((3, NC, 4)),
             dma((4,)),
         ],
         compiler_params=pltpu.CompilerParams(
-            collective_id=0, has_side_effects=True, vmem_limit_bytes=67_000_000
+            collective_id=0, has_side_effects=True, vmem_limit_bytes=60_000_000
         ),
     )(
         tokens.reshape(ROWS, BLK), first_gain[None], mixer_gain[None], second_gain[None], conv_taps, first_gate, first_up, first_down, conv_input, outer_gate,

time: 128 us -> 124 us (0.969)
  Pallas kernels: 126 us -> 123 us
    pallas_call x1, Pallas kernels: 126 us -> 123 us  [on_device(): pl.pallas_call(layer_kernel, out_shape=pltpu.VMEM((ROWS, BLK), BF16), in_...]
where the time goes in v3:
time: 124 us
  Pallas kernels  123 us (99%)
    pallas_call x1, Pallas kernels, on_device(): pl.pallas_call(layer_kernel, out_shape=pltpu.VMEM((ROWS, BLK), BF16), in_...  123 us

profile of v3, /device:TPU:0, one launch (start us, length us, event | category | flops | bytes accessed | tf_op | source)
XLA Modules:
  0.0 124.1 jit_solution(12901493147748091370)
XLA Ops:
  0.0 123.4 %shard_map.145 = bf16[768,256]{1,0:T(8,128)(2,1)S(1)} custom-call(bf16[768,256]{1,0:T(8,128)(2,1)} %bitcast.6, f32[1,2048]{1,0:T(1,128)} %bitcast.7, f32[1,2048]{1,0:T(1,128)} %bitcast.8, f32[1,2048]{1,0:T(1,128)} %bitcast.9, f32[3,128]{1,0:T(4,128)} %taps_in.1, bf16[128,640]{1,0:T(8,128)(2,1)} %fgate.1, bf16[128,640]{1,0:T(8,128)(2,1)} %fup.1, ...), custom_call_target="tpu_custom_call" | custom-call | tf_op jit(solution)/shard_map/pallas_call | solution.py:343
  123.4 0.7 copy.17

commit v4 on v3

--- a/solution.py
+++ b/solution.py
@@ -127,13 +127,13 @@
             rows = pl.ds(64 * h, 64)
         part = w.at[slot(h, a, b), pl.ds(first, count), rows]
         pltpu.make_async_remote_copy(
-            src_ref=part, dst_ref=part, send_sem=w_send.at[g], recv_sem=w_recv.at[g, landing],
+            src_ref=part, dst_ref=part, send_sem=w_send.at[g], recv_sem=w_recv.at[g, landing - 1],
             device_id=w_device(h, phase, d), device_id_type=MESH,
         ).start()
 
     def w_wait(g, landing):
         first, count = GROUPS[g]
-        await_bytes(w.at[pl.ds(0, UNITS[landing]), pl.ds(first, count)], w_recv.at[g, landing])
+        await_bytes(w.at[pl.ds(0, UNITS[landing]), pl.ds(first, count)], w_recv.at[g, landing - 1])
 
     both = [(h, d) for h in (0, 1) for d in (1, 3)]
 
@@ -170,7 +170,7 @@
 
     def y_copy(src, dst, stage, c, recv, device):
         pltpu.make_async_remote_copy(
-            src_ref=src, dst_ref=dst, send_sem=y_send.at[stage, c], recv_sem=recv,
+            src_ref=src, dst_ref=dst, send_sem=y_send.at[stage], recv_sem=recv,
             device_id=device, device_id_type=MESH,
         ).start()
 
@@ -188,28 +188,28 @@
         for landing, parts in ((0, (front(c), rear(c))), (3, (rear(c), front(c)))):
             for part, device in zip(parts, (above, below)):
                 half = xg.at[stage, t, part]
-                y_copy(half, half, stage, c, g_recv.at[stage, c, landing], device)
-        y_copy(ref, ref, stage, c, g_recv.at[stage, c, 2], partner)
+                y_copy(half, half, stage, c, g_recv.at[c, landing], device)
+        y_copy(ref, ref, stage, c, g_recv.at[c, 2], partner)
 
     def gather_1(stage, c):
-        await_bytes(xg.at[stage, 0, rows_of(c)], g_recv.at[stage, c, 0])
+        await_bytes(xg.at[stage, 0, rows_of(c)], g_recv.at[c, 0])
         for block, part, device in ((mine[3], front(c), above), (mine[1], rear(c), below)):
             ref = xg.at[stage, block, part]
-            y_copy(ref, ref, stage, c, g_recv.at[stage, c, 1], device)
+            y_copy(ref, ref, stage, c, g_recv.at[c, 1], device)
 
     def gather_rest(stage, c):
-        await_bytes(xg.at[stage, 0, rows_of(c)], g_recv.at[stage, c, 3])
+        await_bytes(xg.at[stage, 0, rows_of(c)], g_recv.at[c, 3])
         for block in (mine[3], mine[1]):
             ref = xg.at[stage, block, rows_of(c)]
-            y_copy(ref, ref, stage, c, g_recv.at[stage, c, 2], partner)
+            y_copy(ref, ref, stage, c, g_recv.at[c, 2], partner)
 
     def gather_2(stage, c):
-        await_bytes(xg.at[stage, 0, rows_of(c)], g_recv.at[stage, c, 1])
+        await_bytes(xg.at[stage, 0, rows_of(c)], g_recv.at[c, 1])
         ref = xg.at[stage, mine[2], rows_of(c)]
-        y_copy(ref, ref, stage, c, g_recv.at[stage, c, 2], partner)
+        y_copy(ref, ref, stage, c, g_recv.at[c, 2], partner)
 
     def gather_3(stage, c):
-        await_bytes(xg.at[stage, pl.ds(0, 4), rows_of(c)], g_recv.at[stage, c, 2])
+        await_bytes(xg.at[stage, pl.ds(0, 4), rows_of(c)], g_recv.at[c, 2])
 
     def norm(stage, c):
         @pl.loop(0, R // SUB)
@@ -257,14 +257,14 @@
         return jnp.dot(rows, jnp.concatenate(columns, axis=1), preferred_element_type=F32)
 
     def down(stage, c, first, count, landing):
-        products = product(stage, c, [others[AHEAD[i]] for i in range(first, first + count)])
+        ahead = AHEAD[first : first + count]
+        products = product(stage, c, [others[i] for i in ahead] + [mine[i] for i in ahead])
         for i in range(count):
             psend[stage, first + i, rows_of(c), :] = products[:, BLK * i : BLK * (i + 1)].astype(BF16)
         part = pl.ds(first, count)
-        y_copy(psend.at[stage, part, rows_of(c)], precv.at[stage, part, rows_of(c)], stage, c, s_recv.at[stage, c, landing], partner)
-        products = product(stage, c, [mine[AHEAD[i]] for i in range(first, first + count)])
+        y_copy(psend.at[stage, part, rows_of(c)], precv.at[stage, part, rows_of(c)], stage, c, s_recv.at[c, landing], partner)
         for i in range(count):
-            pown[first + i, rows_of(c), :] = products[:, BLK * i : BLK * (i + 1)]
+            pown[first + i, rows_of(c), :] = products[:, BLK * (count + i) : BLK * (count + i + 1)]
 
     def down_first(stage, c):
         down(stage, c, 0, 1, 0)
@@ -276,10 +276,10 @@
         return pown[i, rows, :] + precv[stage, i, rows, :].astype(F32)
 
     def sum_a(stage, c):
-        await_bytes(precv.at[stage, 0, rows_of(c)], s_recv.at[stage, c, 0])
+        await_bytes(precv.at[stage, 0, rows_of(c)], s_recv.at[c, 0])
         s1[stage, rows_of(c), :] = pair_sum(stage, 0, rows_of(c)).astype(BF16)
         for part, device in ((front(c), above), (rear(c), below)):
-            y_copy(s1.at[stage, part], r1.at[stage, part], stage, c, s_recv.at[stage, c, 1], device)
+            y_copy(s1.at[stage, part], r1.at[stage, part], stage, c, s_recv.at[c, 1], device)
 
     def send_halves(stage, c, parts, with_r1):
         for i, part, device in ((1, parts[0], above), (2, parts[1], below)):
@@ -287,18 +287,18 @@
             if with_r1:
                 value = value + r1[stage, part, :].astype(F32)
             s2[stage, i - 1, part, :] = value.astype(BF16)
-            y_copy(s2.at[stage, i - 1, part], r2.at[stage, i - 1, part], stage, c, s_recv.at[stage, c, 2], device)
+            y_copy(s2.at[stage, i - 1, part], r2.at[stage, i - 1, part], stage, c, s_recv.at[c, 2], device)
 
     def sum_early(stage, c):
-        await_bytes(precv.at[stage, pl.ds(1, 3), rows_of(c)], s_recv.at[stage, c, 3])
+        await_bytes(precv.at[stage, pl.ds(1, 3), rows_of(c)], s_recv.at[c, 3])
         send_halves(stage, c, (rear(c), front(c)), False)
 
     def sum_b(stage, c):
-        await_bytes(r1.at[stage, rows_of(c)], s_recv.at[stage, c, 1])
+        await_bytes(r1.at[stage, rows_of(c)], s_recv.at[c, 1])
         send_halves(stage, c, (front(c), rear(c)), True)
 
     def sum_c(stage, c):
-        await_bytes(r2.at[stage, pl.ds(0, 2), rows_of(c)], s_recv.at[stage, c, 2])
+        await_bytes(r2.at[stage, pl.ds(0, 2), rows_of(c)], s_recv.at[c, 2])
 
         rows = rows_of(c)
         branch = pair_sum(stage, 3, rows) + r2[stage, 0, rows, :].astype(F32) + r2[stage, 1, rows, :].astype(F32)
@@ -321,16 +321,21 @@
         W=weights, G0=gather_0, G1=gather_1, GH=gather_rest, G2=gather_2, G3=gather_3, N=norm, F=mid,
         DA=down_first, DB=down_rest, SA=sum_a, SE=sum_early, SB=sum_b, SC=sum_c,
     )
-    for name, a, b in ORDER:
+
+    def sent(stage):
+        for _ in range(2):
+            await_bytes(xg.at[0, pl.ds(0, 7)], y_send.at[stage])
+
+    for step, (name, a, b) in enumerate(ORDER):
+        if step == len(ORDER) - 2:
+            for g, (first, count) in enumerate(GROUPS):
+                await_bytes(w.at[pl.ds(0, 15), pl.ds(first, count)], w_send.at[g])
+            sent(0)
+            sent(1)
         with jax.named_scope(f"{name}_{a}_{b}"):
             tasks[name](a, b)
 
-    for g, (first, count) in enumerate(GROUPS):
-        await_bytes(w.at[pl.ds(0, 15), pl.ds(first, count)], w_send.at[g])
-    for stage in range(3):
-        for c in range(NC):
-            await_bytes(xg.at[0, pl.ds(0, 7), rows_of(c)], y_send.at[stage, c])
-            await_bytes(xg.at[0, pl.ds(0, 7), rows_of(c)], y_send.at[stage, c])
+    sent(2)
 
 
 def on_device(
@@ -365,10 +370,10 @@
             dma((5,)),
             dma,
             dma((5,)),
-            dma((5, 7)),
-            dma((3, NC)),
-            dma((3, NC, 4)),
-            dma((3, NC, 4)),
+            dma((5, 6)),
+            dma((3,)),
+            dma((NC, 4)),
+            dma((NC, 4)),
             dma((4,)),
         ],
         compiler_params=pltpu.CompilerParams(

time: 124 us -> 123 us (level)
    pallas_call x1, Pallas kernels: 123 us -> 122 us  [on_device(): pl.pallas_call(layer_kernel, out_shape=pltpu.VMEM((ROWS, BLK), BF16), in_...]
where the time goes in v4:
time: 123 us; the launch traced here: 122 us
  Pallas kernels  122 us (99%)
    pallas_call x1, Pallas kernels, on_device(): pl.pallas_call(layer_kernel, out_shape=pltpu.VMEM((ROWS, BLK), BF16), in_...  122 us

profile of v4, /device:TPU:0, one launch (start us, length us, event | category | flops | bytes accessed | tf_op | source)
XLA Modules:
  0.0 122.4 jit_solution(11598886549912972213)
XLA Ops:
  0.0 121.6 %shard_map.145 = bf16[768,256]{1,0:T(8,128)(2,1)S(1)} custom-call(bf16[768,256]{1,0:T(8,128)(2,1)} %bitcast.6, f32[1,2048]{1,0:T(1,128)} %bitcast.7, f32[1,2048]{1,0:T(1,128)} %bitcast.8, f32[1,2048]{1,0:T(1,128)} %bitcast.9, f32[3,128]{1,0:T(4,128)} %taps_in.1, bf16[128,640]{1,0:T(8,128)(2,1)} %fgate.1, bf16[128,640]{1,0:T(8,128)(2,1)} %fup.1, ...), custom_call_target="tpu_custom_call" | custom-call | tf_op jit(solution)/shard_map/pallas_call | solution.py:348
  121.6 0.7 copy.17

commit v5 on v4

--- a/solution.py
+++ b/solution.py
@@ -21,7 +21,7 @@
 SUB = 96
 SLABS = 34
 GROUPS = ((0, 10), (10, 5), (15, 4), (19, 10), (29, 5))
-UNITS = (0, 2, 3, 4, 3, 2, 1)
+UNITS = (0, 2, 3, 4, 2, 4)
 AHEAD = (2, 1, 3, 0)
 
 
@@ -91,14 +91,14 @@
         else:
             sources = [conv_in, outer_gate, inner_gate, mix_out]
         first = GROUPS[g][0]
-        return [pltpu.make_async_copy(a, w.at[f, first + i], w_load.at[g]) for i, a in enumerate(sources)]
+        return [pltpu.make_async_copy(a, w.at[f, first + i], w_load.at[min(g, 1)]) for i, a in enumerate(sources)]
 
     def await_bytes(ref, sem):
         pltpu.make_async_copy(ref, ref, sem).wait()
 
     def load_vectors():
-        copies = [pltpu.make_async_copy(a, gains.at[i], k_load.at[i]) for i, a in enumerate((gain_1, gain_2, gain_3))]
-        return copies + [pltpu.make_async_copy(taps_in, taps, k_load.at[3])]
+        copies = [pltpu.make_async_copy(a, gains.at[i], k_load.at[0]) for i, a in enumerate((gain_1, gain_2, gain_3))]
+        return copies + [pltpu.make_async_copy(taps_in, taps, k_load.at[1])]
 
     load_tokens().start()
     for g in range(5):
@@ -115,14 +115,14 @@
     gi[:, pl.ds(0, 8), :] = jnp.zeros((2, 8, 128), F32)
 
     load_tokens().wait()
-    for copy in load_vectors():
-        copy.wait()
+    await_bytes(gains, k_load.at[0])
+    await_bytes(taps, k_load.at[1])
     pl.semaphore_wait(barrier, len(peers))
 
     def w_copy(g, h, a, b, phase, d, quarter, landing):
         first, count = GROUPS[g]
         if quarter:
-            rows = pl.ds(64 * h + (0 if d == 1 else 32), 32)
+            rows = pl.ds(64 * h + (0 if (d == 1) == (quarter == 1) else 32), 32)
         else:
             rows = pl.ds(64 * h, 64)
         part = w.at[slot(h, a, b), pl.ds(first, count), rows]
@@ -140,33 +140,35 @@
     def weights(g, rnd):
         first, count = GROUPS[g]
         if rnd == 0:
-            await_bytes(w.at[f, pl.ds(first, count)], w_load.at[g])
+            if g < 2:
+                loaded = pl.ds(0, 10) if g == 0 else pl.ds(10, SLABS - 10)
+                await_bytes(w.at[f, loaded], w_load.at[g])
             for h, d in both:
-                w_copy(g, h, 0, 0, 1, d, False, 1)
+                w_copy(g, h, 0, 0, 1, d, 0, 1)
             for h, d in both:
-                w_copy(g, h, 0, 0, 2, d, False, 2)
+                w_copy(g, h, 0, 0, 2, d, 0, 2)
         elif rnd == 5:
             w_wait(g, 5)
-            w_wait(g, 6)
         else:
             w_wait(g, rnd)
             for h, d in both:
                 back = 4 - d
                 if rnd == 1:
-                    w_copy(g, h, back, 0, 1, d, True, 2)
+                    w_copy(g, h, back, 0, 1, d, 1, 2)
                 elif rnd == 2:
-                    w_copy(g, h, 0, back, 2, d, True, 4)
+                    w_copy(g, h, 0, back, 2, d, 1, 4)
+                    w_copy(g, h, 2, 0, 2, d, 1, 4)
                 elif rnd == 3:
-                    w_copy(g, h, 1, back, 2, d, True, 5)
-                    w_copy(g, h, 3, back, 2, d, True, 5)
+                    w_copy(g, h, 1, back, 2, d, 1, 5)
+                    w_copy(g, h, 3, back, 2, d, 1, 5)
                 else:
-                    w_copy(g, h, 2, back, 2, d, True, 6)
+                    w_copy(g, h, 2, back, 2, d, 1, 5)
             for h, d in both:
                 if rnd == 1:
-                    w_copy(g, h, 1, 0, 2, d, False, 3)
-                    w_copy(g, h, 3, 0, 2, d, False, 3)
+                    w_copy(g, h, 1, 0, 2, d, 0, 3)
+                    w_copy(g, h, 3, 0, 2, d, 0, 3)
                 elif rnd == 2:
-                    w_copy(g, h, 2, 0, 2, d, False, 4)
+                    w_copy(g, h, 2, 0, 2, d, 2, 5)
 
     def y_copy(src, dst, stage, c, recv, device):
         pltpu.make_async_remote_copy(
@@ -367,14 +369,14 @@
             pltpu.VMEM((ROWS, 128), BF16),
             pltpu.VMEM((3, 1, D), F32),
             pltpu.VMEM((3, 128), F32),
-            dma((5,)),
+            dma((2,)),
             dma,
             dma((5,)),
-            dma((5, 6)),
+            dma((5, 5)),
             dma((3,)),
             dma((NC, 4)),
             dma((NC, 4)),
-            dma((4,)),
+            dma((2,)),
         ],
         compiler_params=pltpu.CompilerParams(
             collective_id=0, has_side_effects=True, vmem_limit_bytes=60_000_000

time: 123 us -> 123 us (level)
  no operation moved by 1% of the time
where the time goes in v5:
time: 123 us; the launch traced here: 122 us
  Pallas kernels  122 us (99%)
    pallas_call x1, Pallas kernels, on_device(): pl.pallas_call(layer_kernel, out_shape=pltpu.VMEM((ROWS, BLK), BF16), in_...  122 us

profile of v5, /device:TPU:0, one launch (start us, length us, event | category | flops | bytes accessed | tf_op | source)
XLA Modules:
  0.0 122.3 jit_solution(16102922370397329996)
XLA Ops:
  0.0 121.5 %shard_map.145 = bf16[768,256]{1,0:T(8,128)(2,1)S(1)} custom-call(bf16[768,256]{1,0:T(8,128)(2,1)} %bitcast.6, f32[1,2048]{1,0:T(1,128)} %bitcast.7, f32[1,2048]{1,0:T(1,128)} %bitcast.8, f32[1,2048]{1,0:T(1,128)} %bitcast.9, f32[3,128]{1,0:T(4,128)} %taps_in.1, bf16[128,640]{1,0:T(8,128)(2,1)} %fgate.1, bf16[128,640]{1,0:T(8,128)(2,1)} %fup.1, ...), custom_call_target="tpu_custom_call" | custom-call | tf_op jit(solution)/shard_map/pallas_call | solution.py:350
  121.5 0.7 copy.17

commit v6 on v5

--- a/solution.py
+++ b/solution.py
@@ -18,7 +18,7 @@
 NC = 4
 R = ROWS // NC
 HALF = R // 2
-SUB = 96
+SUB = 192
 SLABS = 34
 GROUPS = ((0, 10), (10, 5), (15, 4), (19, 10), (29, 5))
 UNITS = (0, 2, 3, 4, 2, 4)

time: 123 us -> 122 us (level)
  no operation moved by 1% of the time
where the time goes in v6:
time: 122 us
  Pallas kernels  122 us (100%)
    pallas_call x1, Pallas kernels, on_device(): pl.pallas_call(layer_kernel, out_shape=pltpu.VMEM((ROWS, BLK), BF16), in_...  122 us

profile of v6, /device:TPU:0, one launch (start us, length us, event | category | flops | bytes accessed | tf_op | source)
XLA Modules:
  0.0 122.3 jit_solution(1300312405044224365)
XLA Ops:
  0.0 121.5 %shard_map.145 = bf16[768,256]{1,0:T(8,128)(2,1)S(1)} custom-call(bf16[768,256]{1,0:T(8,128)(2,1)} %bitcast.6, f32[1,2048]{1,0:T(1,128)} %bitcast.7, f32[1,2048]{1,0:T(1,128)} %bitcast.8, f32[1,2048]{1,0:T(1,128)} %bitcast.9, f32[3,128]{1,0:T(4,128)} %taps_in.1, bf16[128,640]{1,0:T(8,128)(2,1)} %fgate.1, bf16[128,640]{1,0:T(8,128)(2,1)} %fup.1, ...), custom_call_target="tpu_custom_call" | custom-call | tf_op jit(solution)/shard_map/pallas_call | solution.py:350
  121.5 0.7 copy.17
